TPU v7x, 256 devices: a whole 4x4x8 slice. The times are simulated.
256 devices in a mesh: sp: 32 (over z, x), tp: 4 (over y), dp: 2 (over core).
Axes of the slice: x: 4, y: 4, z: 8, core: 2. Of those that a mesh axis runs over, the one named last changes fastest.
Arguments:
- latent: bfloat16 [4, 32768, 2048], P('dp', 'sp'), may hold values from -6 to 6
- context: bfloat16 [4, 1024, 2048], P('dp', 'sp'), may hold values from -6 to 6
- condition: bfloat16 [4, 2048], P('dp', 'sp'), may hold values from -6 to 6
- ctx_cond: bfloat16 [2048], P('sp'), may hold values from -6 to 6
- norm_gain: float32 [2048], replicated, may hold values from 0.1 to 1.9
- w_shift: bfloat16 [2048, 2048], P('sp', 'tp'), may hold values from -0.125 to 0.125
- w_scale: bfloat16 [2048, 2048], P('sp', 'tp'), may hold values from -0.125 to 0.125
- w_gate: bfloat16 [2048, 2048], P('sp', 'tp'), may hold values from -0.125 to 0.125
- w_query: bfloat16 [2048, 1024], P(None, 'tp'), may hold values from -0.125 to 0.125
- w_key: bfloat16 [2048, 256], P(None, 'tp'), may hold values from -0.125 to 0.125
- w_value: bfloat16 [2048, 256], P(None, 'tp'), may hold values from -0.125 to 0.125
- w_out: bfloat16 [1024, 2048], P('tp'), may hold values from -4 to 4
- sink_logit: float32 [16], P('tp'), may hold values from 4 to 7
- ctx_lift: float32 [16], P('tp'), may hold values from -4 to 220
Outputs:
- mixed: bfloat16 [4, 32768, 2048], P('dp', ('sp', 'tp'))
All inputs are finite; a program needn't handle non-finite values.
Results may differ from a plain program's by a relative error of at most 0.012.
Values may be sent and summed in bfloat16 or wider, within the bound.
A program may use at most 128 MiB of HBM per device.

v0:
```python
import jax
import jax.numpy as jnp
from jax import lax
from jax.sharding import PartitionSpec as P

HEAD = 64
WINDOW = 128
GRID_COLS = 64


epsilon = 1e-06
rope_base = 10000.0
masked_value = -1e30


def copy_for_each(array, axis):
    copies = jnp.broadcast_to(array, (lax.axis_size(axis), *array.shape))
    return lax.all_to_all(copies, axis, split_axis=0, concat_axis=0, tiled=True)


def over_copies(array, axis):
    return copy_for_each(array, axis).sum(axis=0)


def in_one(arrays, axis):
    vector, at, done = (jnp.concatenate([a.reshape(-1) for a in arrays]), 0, [])
    so_far = over_copies(vector, axis)
    for a in arrays:
        done.append(so_far[at : at + a.size].reshape(a.shape))
        at += a.size
    return tuple(done)


def sent_together(arrays, axis, dim, along):
    widths = [a.shape[along] for a in arrays]
    both = jnp.concatenate(arrays, axis=along)
    whole = lax.all_gather(both, axis, axis=dim, tiled=True)
    return tuple(jnp.split(whole, [sum(widths[:k]) for k in range(1, len(widths))], axis=along))


def with_halo(cells, sides, width):
    for axis, dim in sides:
        count = lax.axis_size(axis)
        ends = count - 1
        head = lax.slice_in_dim(cells, 0, width, axis=dim)
        tail = lax.slice_in_dim(cells, cells.shape[dim] - width, cells.shape[dim], axis=dim)
        cells = jnp.concatenate(
            [
                lax.ppermute(tail, axis, [(i, (i + 1) % count) for i in range(ends)]),
                cells,
                lax.ppermute(head, axis, [((i + 1) % count, i) for i in range(ends)]),
            ],
            axis=dim,
        )
    return cells


def laid_out(blocks, dim):
    dims = list(blocks.shape[1:])
    dims[dim] *= blocks.shape[0]
    return jnp.moveaxis(blocks, 0, dim).reshape(dims)


def gathered_copies(array, axis, dim):
    return laid_out(copy_for_each(array, axis), dim)


def modulated(inputs, norm_gain, shift_vec, scale_vec):
    widened = inputs.astype(jnp.float32)
    inverse = lax.rsqrt(jnp.mean(widened * widened, axis=-1, keepdims=True) + epsilon)
    return (widened * inverse * norm_gain * (1.0 + scale_vec) + shift_vec).astype(jnp.bfloat16)


def rotate_half(half_part, angles):
    first_half, second = jnp.split(half_part, 2, axis=-1)
    cosine = jnp.cos(angles)[:, None, :]
    sine_part = jnp.sin(angles)[:, None, :]
    return jnp.concatenate(
        [first_half * cosine - second * sine_part, first_half * sine_part + second * cosine],
        axis=-1,
    )


def rotate(inputs, positions):
    quarter = inputs.shape[-1] // 4
    frequency = rope_base ** (-jnp.arange(quarter, dtype=jnp.float32) / quarter)
    row_angle = (positions // GRID_COLS).astype(jnp.float32)[:, None] * frequency
    col_angle = (positions % GRID_COLS).astype(jnp.float32)[:, None] * frequency
    half_size = 2 * quarter
    return jnp.concatenate(
        [
            rotate_half(inputs[..., :half_size], row_angle),
            rotate_half(inputs[..., half_size:], col_angle),
        ],
        axis=-1,
    )


def shards(
    latent,
    context,
    condition,
    ctx_cond,
    norm_gain,
    w_shift,
    w_scale,
    w_gate,
    w_query,
    w_key,
    w_value,
    w_out,
    sink_logit,
    ctx_lift,
):
    samples, tokens, model_width = latent.shape
    head_size = HEAD
    sp_count = lax.axis_size("sp")
    cond_rows = jnp.concatenate([condition, ctx_cond[None, :]], axis=0)
    active = jax.nn.silu(cond_rows.astype(jnp.float32)).astype(jnp.bfloat16)
    shift_part, scale_part, gate_part = in_one(
        (
            jnp.dot(active, w_shift, preferred_element_type=jnp.float32),
            jnp.dot(active, w_scale, preferred_element_type=jnp.float32),
            jnp.dot(active, w_gate, preferred_element_type=jnp.float32),
        ),
        "sp",
    )
    shift_vec, scale_vec, gate_vec = sent_together((shift_part, scale_part, gate_part), "tp", 1, 0)
    hidden = modulated(
        latent, norm_gain, shift_vec[:samples, None, :], scale_vec[:samples, None, :]
    )
    offset_row = lax.axis_index("sp") * tokens
    positions = offset_row + jnp.arange(tokens, dtype=jnp.int32)
    query_heads = w_query.shape[1] // head_size
    key_heads = w_key.shape[1] // head_size
    group_size = query_heads // key_heads
    keyed = key_heads * head_size
    queries = rotate(
        jnp.einsum("snd,dc->snc", hidden, w_query, preferred_element_type=jnp.float32).reshape(
            samples, tokens, query_heads, head_size
        ),
        positions,
    ).astype(jnp.bfloat16)
    key_rows = rotate(
        jnp.einsum("snd,dc->snc", hidden, w_key, preferred_element_type=jnp.float32).reshape(
            samples, tokens, key_heads, head_size
        ),
        positions,
    ).astype(jnp.bfloat16)
    values = jnp.einsum("snd,dc->snc", hidden, w_value, preferred_element_type=jnp.float32).astype(
        jnp.bfloat16
    )
    local_pairs = jnp.concatenate([key_rows.reshape(samples, tokens, keyed), values], axis=-1)
    extended = with_halo(local_pairs, (("sp", 1),), WINDOW)
    ctx_hidden = modulated(context, norm_gain, shift_vec[samples], scale_vec[samples])
    ctx_keys = jnp.einsum(
        "snd,dc->snc", ctx_hidden, w_key, preferred_element_type=jnp.float32
    ).astype(jnp.bfloat16)
    ctx_values = jnp.einsum(
        "snd,dc->snc", ctx_hidden, w_value, preferred_element_type=jnp.float32
    ).astype(jnp.bfloat16)
    context_pairs = gathered_copies(jnp.concatenate([ctx_keys, ctx_values], axis=-1), "sp", 1)
    block_rows = min(512, tokens)
    blocks = tokens // block_rows
    span_rows = block_rows + 2 * WINDOW
    latent_len = tokens * sp_count
    lift_rows = ctx_lift.reshape(key_heads, group_size, 1, 1)
    sink_rows = sink_logit.reshape(key_heads, group_size, 1, 1)
    factor = head_size ** (-0.5)

    def attend(step_id):
        sample = step_id // blocks
        row_start = step_id % blocks * block_rows
        q_rows = lax.dynamic_slice_in_dim(
            lax.dynamic_index_in_dim(queries, sample, 0, keepdims=False), row_start, block_rows, 0
        )
        q_rows = q_rows.reshape(block_rows, key_heads, group_size, head_size)
        pair_rows = lax.dynamic_slice_in_dim(
            lax.dynamic_index_in_dim(extended, sample, 0, keepdims=False), row_start, span_rows, 0
        )
        near_keys = pair_rows[:, :keyed].reshape(span_rows, key_heads, head_size)
        near_values = pair_rows[:, keyed:].reshape(span_rows, key_heads, head_size)
        ctx_rows = lax.dynamic_index_in_dim(context_pairs, sample, 0, keepdims=False)
        far_keys = ctx_rows[:, :keyed].reshape(-1, key_heads, head_size)
        far_values = ctx_rows[:, keyed:].reshape(-1, key_heads, head_size)
        query_pos = offset_row + row_start + jnp.arange(block_rows, dtype=jnp.int32)
        key_pos = offset_row + row_start - WINDOW + jnp.arange(span_rows, dtype=jnp.int32)
        inside = (
            (key_pos[None, :] >= 0)
            & (key_pos[None, :] < latent_len)
            & (jnp.abs(query_pos[:, None] - key_pos[None, :]) <= WINDOW)
        )
        near_scores = (
            jnp.einsum("qgrd,kgd->grqk", q_rows, near_keys, preferred_element_type=jnp.float32)
            * factor
        )
        near_scores = jnp.where(inside[None, None], near_scores, masked_value)
        far_scores = (
            jnp.einsum("qgrd,kgd->grqk", q_rows, far_keys, preferred_element_type=jnp.float32)
            * factor
            + lift_rows
        )
        row_max = jnp.maximum(
            jnp.maximum(near_scores.max(-1, keepdims=True), far_scores.max(-1, keepdims=True)),
            sink_rows,
        )
        near_exp = jnp.exp(near_scores - row_max)
        far_exp = jnp.exp(far_scores - row_max)
        normaliser = (
            near_exp.sum(-1, keepdims=True)
            + far_exp.sum(-1, keepdims=True)
            + jnp.exp(sink_rows - row_max)
        )
        outcome = jnp.einsum(
            "grqk,kgd->qgrd",
            (near_exp / normaliser).astype(jnp.bfloat16),
            near_values,
            preferred_element_type=jnp.float32,
        )
        outcome = outcome + jnp.einsum(
            "grqk,kgd->qgrd",
            (far_exp / normaliser).astype(jnp.bfloat16),
            far_values,
            preferred_element_type=jnp.float32,
        )
        return outcome.astype(jnp.bfloat16).reshape(block_rows, query_heads * head_size)

    attended = lax.map(attend, jnp.arange(samples * blocks, dtype=jnp.int32)).reshape(
        samples, tokens, query_heads * head_size
    )
    by_rows = lax.all_to_all(attended, "tp", split_axis=1, concat_axis=2, tiled=True)
    projected = jnp.einsum(
        "snc,cd->snd",
        by_rows,
        lax.all_gather(w_out, "tp", axis=0, tiled=True),
        preferred_element_type=jnp.float32,
    )
    return (gate_vec[:samples, None, :] * projected).astype(jnp.bfloat16)


def solution(mesh):
    return jax.shard_map(
        shards,
        mesh=mesh,
        in_specs=(
            P("dp", "sp", None),
            P("dp", "sp", None),
            P("dp", "sp"),
            P("sp"),
            P(),
            P("sp", "tp"),
            P("sp", "tp"),
            P("sp", "tp"),
            P(None, "tp"),
            P(None, "tp"),
            P(None, "tp"),
            P("tp", None),
            P("tp"),
            P("tp"),
        ),
        out_specs=P("dp", ("sp", "tp"), None),
        check_vma=False,
    )
```

profile of v0, /device:TPU:32, one launch (start us, length us, event | category | flops | bytes accessed | tf_op | source)
XLA Modules:
  0.0 216.5 jit_solution(1232252963164538009)
XLA Ops:
  10.8 11.2 %all-to-all-start = ((f32[32,1,4608]{2,1,0:T(1,128)}), f32[32,1,4608]{2,1,0:T(1,128)S(1)}, u32[]{:S(2)}, u32[]{:S(2)}) async-start(f32[32,1,4608]{2,1,0:T(1,128)} %broadcast_in_dim.36), calls=%async_computation | async-start | bytes 1179648 | tf_op jit(solution)/shard_map/all_to_all | solution.py:18
  23.9 5.1 %fusion.26 = f32[2,1024]{1,0:T(2,128)S(1)} fusion(bf16[2,1024,2048]{2,1,0:T(8,128)(2,1)} %param.16), kind=kLoop, calls=%fused_computation.44 | loop fusion | flops 12580864 | bytes 8396800 | tf_op jit(solution)/shard_map/reduce_sum | solution.py:70
  29.6 10.9 %all-to-all-done = f32[32,1,4608]{2,1,0:T(1,128)S(1)} async-done(((f32[32,1,4608]{2,1,0:T(1,128)}), f32[32,1,4608]{2,1,0:T(1,128)S(1)}, u32[]{:S(2)}, u32[]{:S(2)}) %all-to-all-start) | async-done | bytes 589856 | tf_op jit(solution)/shard_map/all_to_all | solution.py:18
  40.9 13.5 %all_gather.6 = f32[9,2048]{1,0:T(8,128)S(1)} all-gather(f32[9,512]{1,0:T(8,128)S(1)} %pad_maximum_fusion.2), channel_id=1, replica_groups=mesh['sp'=32,'tp'=4,'dp'=2] {'tp'}, dimensions={1}, use_global_device_ids=true | all-gather | bytes 92160 | tf_op jit(solution)/shard_map/all_gather | solution.py:37
  55.1 8.7 %fusion.36 = f32[2,1024,256]{1,2,0:T(8,128)} fusion(bf16[2048,256]{1,0:T(8,128)(2,1)S(1)} %copy-done, bf16[2,1024,2048]{2,1,0:T(8,128)(2,1)} %param.16, f32[2,2048]{1,0:T(2,128)S(1)} %get-tuple-element.227, f32[2,2048]{1,0:T(2,128)S(1)} %get-tuple-element.228, f32[2048]{0:T(1024)S(1)} %copy-done.9, f32[2,1024]{1,0:T(2,128)S(1)} %add_rsqrt_fusion), kind=kOutput, calls=%fused_computation.58 | convolution fusion | flops 2172649472 | bytes 11583488 | tf_op jit(solution)/shard_map/snd,dc->snc/dot_general | solution.py:139
  63.8 6.1 %convolution_bitcast_fusion = f32[2,1024,1,64]{1,3,0,2:T(8,128)S(1)} fusion(bf16[2,1024,2048]{2,1,0:T(8,128)(2,1)} %param.16, f32[2,2048]{1,0:T(2,128)S(1)} %get-tuple-element.227, f32[2,2048]{1,0:T(2,128)S(1)} %get-tuple-element.228, f32[2048]{0:T(1024)S(1)} %copy-done.9, f32[2,1024]{1,0:T(2,128)S(1)} %add_rsqrt_fusion, bf16[2048,64]{0,1:T(8,128)(2,1)S(1)} %copy-done.7), kind=kOutput, calls=%fused_computation.52 | convolution fusion | flops 562036736 | bytes 9224192 | tf_op jit(solution)/shard_map/snd,dc->snc/dot_general | solution.py:145
  71.7 4.8 %all-to-all-start.1 = ((bf16[32,2,32,128]{3,2,1,0:T(8,128)(2,1)}), bf16[32,2,32,128]{3,2,1,0:T(8,128)(2,1)S(1)}, u32[]{:S(2)}, u32[]{:S(2)}) async-start(bf16[32,2,32,128]{3,2,1,0:T(8,128)(2,1)} %broadcast_in_dim.68), calls=%async_computation.1 | async-start | bytes 1048576 | tf_op jit(solution)/shard_map/all_to_all | solution.py:18
  76.5 7.1 %fusion.35 = bf16[2,1024,128]{1,2,0:T(8,128)(2,1)S(1)} fusion(bf16[2,1024,128]{1,2,0:T(8,128)(2,1)S(1)} %fusion.59, bf16[2,1024,2048]{2,1,0:T(8,128)(2,1)} %param.16, f32[2,2048]{1,0:T(2,128)S(1)} %get-tuple-element.227, f32[2,2048]{1,0:T(2,128)S(1)} %get-tuple-element.228, f32[2048]{0:T(1024)S(1)} %copy-done.9, f32[2,1024]{1,0:T(2,128)S(1)} %add_rsqrt_fusion, ...), kind=kOutput, calls=%fused_computation.54 | convolution fusion | flops 562167808 | bytes 8962048 | tf_op jit(solution)/shard_map/snd,dc->snc/dot_general | solution.py:150
  83.7 3.4 %collective-permute-start = (bf16[2,128,128]{1,2,0:T(8,128)(2,1)S(1)}, bf16[2,128,128]{1,2,0:T(8,128)(2,1)S(1)}, u32[]{:S(2)}, u32[]{:S(2)}) collective-permute-start(bf16[2,128,128]{1,2,0:T(8,128)(2,1)S(1)} %get-tuple-element.224), channel_id=1, source_target_pairs={{0,8},{8,16},{16,24},{24,32},{32,40},{40,48},{48,56},{56,64},{64,7... | collective-permute-start | bytes 196616 | tf_op jit(solution)/shard_map/ppermute | solution.py:49
  87.0 4.6 %collective-permute-start.1 = (bf16[2,128,128]{1,2,0:T(8,128)(2,1)S(1)}, bf16[2,128,128]{1,2,0:T(8,128)(2,1)S(1)}, u32[]{:S(2)}, u32[]{:S(2)}) collective-permute-start(bf16[2,128,128]{1,2,0:T(8,128)(2,1)S(1)} %get-tuple-element.225), channel_id=1, source_target_pairs={{8,0},{16,8},{24,16},{32,24},{40,32},{48,40},{56,48},{64,56},{72,6... | collective-permute-start | bytes 196616 | tf_op jit(solution)/shard_map/ppermute | solution.py:51
  95.5 91.0 %while.13 = (s32[]{:T(128)}, bf16[4,512,256]{2,1,0:T(8,128)(2,1)}, s32[4]{0:T(128)S(1)}, bf16[2,1280,128]{1,2,0:T(8,128)(2,1)}, s32[]{:T(128)}, /*index=5*/bf16[...) while((s32[]{:T(128)}, bf16[4,512,256]{2,1,0:T(8,128)(2,1)}, ...), condition=%wide.region_8.9_spmd, body=%wide.region_3.8_spmd.sunk | while | flops 985405696 | bytes 75716256 | solution.py:228
  98.9 4.6 %bitcast_reduce_fusion.2 = (f32[4,512]{1,0:T(4,128)S(1)}, f32[1024,512,4]{1,0,2:T(8,128)}) fusion(f32[4]{0:T(128)S(1)} %bitcast.200, bf16[2,1024,4,64]{1,3,2,0:T(8,128)(2,1)S(1)} %get-tuple-element.344, s32[]{:T(128)S(6)} %select_n.121, s32[]{:T(128)S(6)} %select_n.124, bf16[1024,128]{0,1:T(8,128)(2,1)S(1)} %bitcast.191), kind=kOutput, calls=%fused_computation.1.clone.1 | convolution fusion | flops 274724864 | bytes 8790536 | tf_op jit(solution)/shard_map/while/body/eval_jaxpr/qgrd,kgd->grqk/dot_general | solution.py:199
  106.5 5.2 %fusion.96 = f32[4,512]{1,0:T(4,128)S(1)} fusion(f32[1024,512,4]{1,0,2:T(8,128)} %get-tuple-element.301, f32[4,512]{1,0:T(4,128)S(1)} %maximum_maximum_fusion.2, f32[4]{0:T(128)S(1)} %bitcast.201), kind=kLoop, calls=%fused_computation.5.clone.1 | loop fusion | flops 8386560 | bytes 8405008 | tf_op jit(solution)/shard_map/while/body/eval_jaxpr/reduce_sum | solution.py:211
  113.3 2.1 fusion.97
  121.7 4.6 %bitcast_reduce_fusion.2 = (f32[4,512]{1,0:T(4,128)S(1)}, f32[1024,512,4]{1,0,2:T(8,128)}) fusion(f32[4]{0:T(128)S(1)} %bitcast.200, bf16[2,1024,4,64]{1,3,2,0:T(8,128)(2,1)S(1)} %get-tuple-element.344, s32[]{:T(128)S(6)} %select_n.121, s32[]{:T(128)S(6)} %select_n.124, bf16[1024,128]{0,1:T(8,128)(2,1)S(1)} %bitcast.191), kind=kOutput, calls=%fused_computation.1.clone.1 | convolution fusion | flops 274724864 | bytes 8790536 | tf_op jit(solution)/shard_map/while/body/eval_jaxpr/qgrd,kgd->grqk/dot_general | solution.py:199
  129.3 5.2 %fusion.96 = f32[4,512]{1,0:T(4,128)S(1)} fusion(f32[1024,512,4]{1,0,2:T(8,128)} %get-tuple-element.301, f32[4,512]{1,0:T(4,128)S(1)} %maximum_maximum_fusion.2, f32[4]{0:T(128)S(1)} %bitcast.201), kind=kLoop, calls=%fused_computation.5.clone.1 | loop fusion | flops 8386560 | bytes 8405008 | tf_op jit(solution)/shard_map/while/body/eval_jaxpr/reduce_sum | solution.py:211
  136.0 2.1 fusion.97
  144.4 4.6 %bitcast_reduce_fusion.2 = (f32[4,512]{1,0:T(4,128)S(1)}, f32[1024,512,4]{1,0,2:T(8,128)}) fusion(f32[4]{0:T(128)S(1)} %bitcast.200, bf16[2,1024,4,64]{1,3,2,0:T(8,128)(2,1)S(1)} %get-tuple-element.344, s32[]{:T(128)S(6)} %select_n.121, s32[]{:T(128)S(6)} %select_n.124, bf16[1024,128]{0,1:T(8,128)(2,1)S(1)} %bitcast.191), kind=kOutput, calls=%fused_computation.1.clone.1 | convolution fusion | flops 274724864 | bytes 8790536 | tf_op jit(solution)/shard_map/while/body/eval_jaxpr/qgrd,kgd->grqk/dot_general | solution.py:199
  152.0 5.2 %fusion.96 = f32[4,512]{1,0:T(4,128)S(1)} fusion(f32[1024,512,4]{1,0,2:T(8,128)} %get-tuple-element.301, f32[4,512]{1,0:T(4,128)S(1)} %maximum_maximum_fusion.2, f32[4]{0:T(128)S(1)} %bitcast.201), kind=kLoop, calls=%fused_computation.5.clone.1 | loop fusion | flops 8386560 | bytes 8405008 | tf_op jit(solution)/shard_map/while/body/eval_jaxpr/reduce_sum | solution.py:211
  167.2 4.6 %bitcast_reduce_fusion.2 = (f32[4,512]{1,0:T(4,128)S(1)}, f32[1024,512,4]{1,0,2:T(8,128)}) fusion(f32[4]{0:T(128)S(1)} %bitcast.200, bf16[2,1024,4,64]{1,3,2,0:T(8,128)(2,1)S(1)} %get-tuple-element.344, s32[]{:T(128)S(6)} %select_n.121, s32[]{:T(128)S(6)} %select_n.124, bf16[1024,128]{0,1:T(8,128)(2,1)S(1)} %bitcast.191), kind=kOutput, calls=%fused_computation.1.clone.1 | convolution fusion | flops 274724864 | bytes 8790536 | tf_op jit(solution)/shard_map/while/body/eval_jaxpr/qgrd,kgd->grqk/dot_general | solution.py:199
  174.8 5.2 %fusion.96 = f32[4,512]{1,0:T(4,128)S(1)} fusion(f32[1024,512,4]{1,0,2:T(8,128)} %get-tuple-element.301, f32[4,512]{1,0:T(4,128)S(1)} %maximum_maximum_fusion.2, f32[4]{0:T(128)S(1)} %bitcast.201), kind=kLoop, calls=%fused_computation.5.clone.1 | loop fusion | flops 8386560 | bytes 8405008 | tf_op jit(solution)/shard_map/while/body/eval_jaxpr/reduce_sum | solution.py:211
  186.5 2.3 %copy.50 = bf16[2,1024,256]{2,0,1:T(2,128)(2,1)S(1)} copy(bf16[2,1024,256]{2,1,0:T(8,128)(2,1)} %bitcast.197) | data formatting | bytes 2097152 | tf_op jit(solution)/shard_map/reshape | solution.py:228
  188.9 14.6 %all_to_all.29 = bf16[2,1024,256]{2,0,1:T(2,128)(2,1)S(1)} all-to-all(bf16[2,1024,256]{2,0,1:T(2,128)(2,1)S(1)} %copy.50), channel_id=1, replica_groups=mesh['sp'=32,'tp'=4,'dp'=2] {'tp'}, dimensions={1} | all-to-all | bytes 2097152 | tf_op jit(solution)/shard_map/all_to_all | solution.py:231
  203.8 5.8 %multiply_convert_fusion = bf16[2,256,2048]{2,1,0:T(8,128)(2,1)} fusion(bf16[2,256,1024]{2,1,0:T(8,128)(2,1)S(1)} %bitcast.198, bf16[1024,2048]{1,0:T(8,128)(2,1)} %all-gather.2.cloned.1.call-done, f32[2,2048]{1,0:T(2,128)S(1)} %copy-done.6), kind=kOutput, calls=%fused_computation.51 | convolution fusion | flops 2149580800 | bytes 7356416 | tf_op jit(solution)/shard_map/snc,cd->snd/dot_general | solution.py:232
  (147 shorter events, 50.4 us)
Async XLA Ops:
  6.5 48.6 %copy-start = (bf16[2048,256]{1,0:T(8,128)(2,1)S(1)}, bf16[2048,256]{1,0:T(8,128)(2,1)}, u32[]{:S(2)}) copy-start(bf16[2048,256]{1,0:T(8,128)(2,1)} %param.24) | copy-start | bytes 3145732
  6.5 48.6 %copy-start.9 = (f32[2048]{0:T(1024)S(1)}, f32[2048]{0:T(1024)}, u32[]{:S(2)}) copy-start(f32[2048]{0:T(1024)} %param.20) | copy-start | bytes 24580
  10.8 29.7 %all-to-all-start = ((f32[32,1,4608]{2,1,0:T(1,128)}), f32[32,1,4608]{2,1,0:T(1,128)S(1)}, u32[]{:S(2)}, u32[]{:S(2)}) async-start(f32[32,1,4608]{2,1,0:T(1,128)} %broadcast_in_dim.36), calls=%async_computation | async-start | bytes 1179648 | tf_op jit(solution)/shard_map/all_to_all | solution.py:18
  22.0 181.7 %all-gather.2.cloned.1.call-start = ((), (), s32[]{:S(2)}) async-start(), calls=%async_computation.3 | async-start | bytes 5242880 | tf_op jit(solution)/shard_map/all_gather | solution.py:235
  55.1 8.7 %copy-start.7 = (bf16[2048,64]{0,1:T(8,128)(2,1)S(1)}, bf16[2048,64]{0,1:T(8,128)(2,1)}, u32[]{:S(2)}) copy-start(bf16[2048,64]{0,1:T(8,128)(2,1)} %param.25) | copy-start | bytes 786436
  63.8 6.2 %copy-start.3 = (bf16[2,32,2048]{2,1,0:T(8,128)(2,1)S(1)}, bf16[2,32,2048]{2,1,0:T(8,128)(2,1)}, u32[]{:S(2)}) copy-start(bf16[2,32,2048]{2,1,0:T(8,128)(2,1)} %param.17) | copy-start | bytes 786436
  63.8 6.5 %copy-start.8 = (bf16[2048,64]{0,1:T(8,128)(2,1)S(1)}, bf16[2048,64]{0,1:T(8,128)(2,1)}, u32[]{:S(2)}) copy-start(bf16[2048,64]{0,1:T(8,128)(2,1)} %param.26) | copy-start | bytes 786436
  71.7 23.7 %all-to-all-start.1 = ((bf16[32,2,32,128]{3,2,1,0:T(8,128)(2,1)}), bf16[32,2,32,128]{3,2,1,0:T(8,128)(2,1)S(1)}, u32[]{:S(2)}, u32[]{:S(2)}) async-start(bf16[32,2,32,128]{3,2,1,0:T(8,128)(2,1)} %broadcast_in_dim.68), calls=%async_computation.1 | async-start | bytes 1048576 | tf_op jit(solution)/shard_map/all_to_all | solution.py:18
  76.5 15.1 %copy-start.1 = (f32[2,1024,256]{1,2,0:T(8,128)S(1)}, f32[2,1024,256]{1,2,0:T(8,128)}, u32[]{:S(2)}) copy-start(f32[2,1024,256]{1,2,0:T(8,128)} %fusion.36) | copy-start | bytes 6291460
  76.5 19.0 %copy-start.4 = (f32[4]{0:T(128)S(1)}, f32[4]{0:T(128)}, u32[]{:S(2)}) copy-start(f32[4]{0:T(128)} %param.29) | copy-start | bytes 52
  76.5 19.0 %copy-start.5 = (f32[4]{0:T(128)S(1)}, f32[4]{0:T(128)}, u32[]{:S(2)}) copy-start(f32[4]{0:T(128)} %param.28) | copy-start | bytes 52
  83.6 8.4 %copy-start.2 = (bf16[2,1024,128]{1,2,0:T(8,128)(2,1)}, bf16[2,1024,128]{1,2,0:T(8,128)(2,1)S(1)}, u32[]{:S(2)}) copy-start(bf16[2,1024,128]{1,2,0:T(8,128)(2,1)S(1)} %fusion.35) | copy-start | bytes 1572868
  83.7 8.4 %collective-permute-start = (bf16[2,128,128]{1,2,0:T(8,128)(2,1)S(1)}, bf16[2,128,128]{1,2,0:T(8,128)(2,1)S(1)}, u32[]{:S(2)}, u32[]{:S(2)}) collective-permute-start(bf16[2,128,128]{1,2,0:T(8,128)(2,1)S(1)} %get-tuple-element.224), channel_id=1, source_target_pairs={{0,8},{8,16},{16,24},{24,32},{32,40},{40,48},{48,56},{56,64},{64,7... | collective-permute-start | bytes 196616 | tf_op jit(solution)/shard_map/ppermute | solution.py:49
  87.0 6.5 %collective-permute-start.1 = (bf16[2,128,128]{1,2,0:T(8,128)(2,1)S(1)}, bf16[2,128,128]{1,2,0:T(8,128)(2,1)S(1)}, u32[]{:S(2)}, u32[]{:S(2)}) collective-permute-start(bf16[2,128,128]{1,2,0:T(8,128)(2,1)S(1)} %get-tuple-element.225), channel_id=1, source_target_pairs={{8,0},{16,8},{24,16},{32,24},{40,32},{48,40},{56,48},{64,56},{72,6... | collective-permute-start | bytes 196616 | tf_op jit(solution)/shard_map/ppermute | solution.py:51
  106.4 6.8 %slice-start = ((s8[8388608]{0:T(1024)(128)(4,1)}), s8[4194304]{0:T(1024)(128)(4,1)S(1)}, s32[]{:S(2)}) async-start(s8[8388608]{0:T(1024)(128)(4,1)} %bitcast.189), calls=%async_computation.4 | async-start | bytes 8388608 | tf_op jit(solution)/shard_map/while
  106.5 6.7 %slice-start.1 = ((s8[8388608]{0:T(1024)(128)(4,1)}), s8[4194304]{0:T(1024)(128)(4,1)S(1)}, s32[]{:S(2)}) async-start(s8[8388608]{0:T(1024)(128)(4,1)} %bitcast.189), calls=%async_computation.5 | async-start | bytes 8388608 | tf_op jit(solution)/shard_map/while
  129.2 6.8 %slice-start = ((s8[8388608]{0:T(1024)(128)(4,1)}), s8[4194304]{0:T(1024)(128)(4,1)S(1)}, s32[]{:S(2)}) async-start(s8[8388608]{0:T(1024)(128)(4,1)} %bitcast.189), calls=%async_computation.4 | async-start | bytes 8388608 | tf_op jit(solution)/shard_map/while
  129.3 6.7 %slice-start.1 = ((s8[8388608]{0:T(1024)(128)(4,1)}), s8[4194304]{0:T(1024)(128)(4,1)S(1)}, s32[]{:S(2)}) async-start(s8[8388608]{0:T(1024)(128)(4,1)} %bitcast.189), calls=%async_computation.5 | async-start | bytes 8388608 | tf_op jit(solution)/shard_map/while
  152.0 6.8 %slice-start = ((s8[8388608]{0:T(1024)(128)(4,1)}), s8[4194304]{0:T(1024)(128)(4,1)S(1)}, s32[]{:S(2)}) async-start(s8[8388608]{0:T(1024)(128)(4,1)} %bitcast.189), calls=%async_computation.4 | async-start | bytes 8388608 | tf_op jit(solution)/shard_map/while
  152.0 6.7 %slice-start.1 = ((s8[8388608]{0:T(1024)(128)(4,1)}), s8[4194304]{0:T(1024)(128)(4,1)S(1)}, s32[]{:S(2)}) async-start(s8[8388608]{0:T(1024)(128)(4,1)} %bitcast.189), calls=%async_computation.5 | async-start | bytes 8388608 | tf_op jit(solution)/shard_map/while
  174.7 6.8 %slice-start = ((s8[8388608]{0:T(1024)(128)(4,1)}), s8[4194304]{0:T(1024)(128)(4,1)S(1)}, s32[]{:S(2)}) async-start(s8[8388608]{0:T(1024)(128)(4,1)} %bitcast.189), calls=%async_computation.4 | async-start | bytes 8388608 | tf_op jit(solution)/shard_map/while
  174.8 6.7 %slice-start.1 = ((s8[8388608]{0:T(1024)(128)(4,1)}), s8[4194304]{0:T(1024)(128)(4,1)S(1)}, s32[]{:S(2)}) async-start(s8[8388608]{0:T(1024)(128)(4,1)} %bitcast.189), calls=%async_computation.5 | async-start | bytes 8388608 | tf_op jit(solution)/shard_map/while
  186.5 17.2 %copy-start.6 = (f32[2,2048]{1,0:T(2,128)S(1)}, f32[2,2048]{1,0:T(2,128)}, u32[]{:S(2)}) copy-start(f32[2,2048]{1,0:T(2,128)} %get-tuple-element.226) | copy-start | bytes 49156
Sparse Core Ops, SparseCore 0:
  24.6 53.0 all-gather.1
where the time goes:
time: 221 us; the launch traced here: 216 us
  matrix products  71.6 us (32%)
  other arithmetic  39.5 us (18%)
  blocking collectives  28.1 us (13%)
  starting transfers between devices  24 us (11%)
  local copies, waits for them, and re-layouts  15.7 us (7%)
  between operations  13.7 us (6%)
  waiting for transfers between devices  13.1 us (6%)
  loops' own time  10.8 us (5%)
    reduce_sum x4, other arithmetic, attend(): far_exp.sum(-1, keepdims=True)  21 us
    dot_general x4, matrix products, attend(): jnp.einsum('qgrd,kgd->grqk', q_rows, far_keys, preferred_element_type=jnp...  18.2 us
    all_to_all x2, starting transfers between devices, copy_for_each(): return lax.all_to_all(copies, axis, split_axis=0, concat_axis=0, tiled=True)  16 us
    all_to_all x1, blocking collectives, shards(): lax.all_to_all(attended, 'tp', split_axis=1, concat_axis=2, tiled=True)  14.6 us
    all_gather x1, blocking collectives, sent_together(): whole = lax.all_gather(both, axis, axis=dim, tiled=True)  13.5 us
    all_to_all x2, waiting for transfers between devices, copy_for_each(): return lax.all_to_all(copies, axis, split_axis=0, concat_axis=0, tiled=True)  11 us
    another operation x1, loops' own time, shards(): lax.map(attend, jnp.arange(samples * blocks, dtype=jnp.int32))  10.8 us
    dot_general x1, matrix products, shards(): jnp.einsum('snd,dc->snc', hidden, w_query, preferred_element_type=jnp.flo...  8.69 us
  transfers between devices with their start and end apart: 5, of which 2 were waited for; matrix products, arithmetic and copies ran while one was open for 54% of the time, Pallas kernels for 0%

commit v1 on v0

v1 whole, which is shorter than its diff:
```python
import functools
import math

import jax
import jax.numpy as jnp
from jax import lax
from jax.experimental import pallas as pl
from jax.experimental.pallas import tpu as pltpu
from jax.sharding import PartitionSpec as P

HEAD = 64
WINDOW = 128
GRID_COLS = 64
EPSILON = 1e-06
ROPE_BASE = 10000.0
NEGATIVE = -1e30
LOG2E = math.log2(math.e)
LANES = 128
MESH = pl.DeviceIdType.MESH
f32 = jnp.float32
bf16 = jnp.bfloat16


def lanes_of(rows):
    return lax.broadcasted_iota(jnp.int32, (rows, LANES), 1)


def drain(ref, sem):
    pltpu.make_async_copy(ref, ref, sem).wait()


def swapped(u, lane):
    return jnp.where(lane % 32 < 16, pltpu.roll(u, LANES - 16, 1), pltpu.roll(u, 16, 1))


def prepare(pairs, kt_ref, v4_ref, sample, start, rows):
    wide = pairs.astype(f32)
    turned = pltpu.roll(wide, HEAD, 1)
    low = lanes_of(rows) < HEAD
    kt_ref[sample, :, pl.ds(start, rows)] = jnp.where(low, wide, turned).astype(bf16).T
    v4_ref[sample, pl.ds(start, rows), :LANES] = jnp.where(low, turned, 1.0).astype(bf16)
    v4_ref[sample, pl.ds(start, rows), LANES:] = jnp.where(low, 1.0, wide).astype(bf16)


def attend(sample, row, near_start, left_off, right_off, qp_ref, kt_ref, v4_ref, lift_ref, sink_ref, att_ref, ctx):
    rows = WINDOW
    q = jnp.concatenate([qp_ref[sample, h, pl.ds(row, rows), :] for h in range(4)], axis=0)
    far_keys = kt_ref[sample, :, :ctx]
    near_keys = kt_ref[sample, :, pl.ds(near_start, 3 * WINDOW)]
    far_all = jnp.dot(q, far_keys, preferred_element_type=f32)
    near_all = jnp.dot(q, near_keys, preferred_element_type=f32)
    qi = lax.broadcasted_iota(jnp.int32, (rows, WINDOW), 0)
    kj = lax.broadcasted_iota(jnp.int32, (rows, WINDOW), 1)
    low = lanes_of(rows) < HEAD
    results = []
    for h in range(4):
        lift = lift_ref[h] * LOG2E
        sink = sink_ref[h] * LOG2E
        part = slice(h * rows, (h + 1) * rows)
        far = far_all[part]
        first = jnp.where(kj >= qi, near_all[part, :WINDOW], NEGATIVE) + left_off
        middle = near_all[part, WINDOW : 2 * WINDOW]
        last = jnp.where(kj <= qi, near_all[part, 2 * WINDOW :], NEGATIVE) + right_off
        near_top = jnp.maximum(jnp.maximum(first, middle), last)
        far_top = jnp.max(far, axis=1, keepdims=True) + lift
        top = jnp.maximum(jnp.maximum(jnp.max(near_top, axis=1, keepdims=True), far_top), sink)
        far_exp = jnp.exp2(far - (top - lift)).astype(bf16)
        near_exp = jnp.concatenate(
            [jnp.exp2(first - top), jnp.exp2(middle - top), jnp.exp2(last - top)], axis=1
        ).astype(bf16)
        cols = slice(0, LANES) if h % 2 == 0 else slice(LANES, 2 * LANES)
        total = jnp.dot(far_exp, v4_ref[sample, :ctx, cols], preferred_element_type=f32) + jnp.dot(
            near_exp, v4_ref[sample, pl.ds(near_start, 3 * WINDOW), cols], preferred_element_type=f32
        )
        weight = pltpu.roll(total, HEAD, 1) + jnp.exp2(sink - top)
        results.append(total / weight)
    for pair in range(2):
        att_ref[sample, pl.ds(row, rows), pair * LANES : (pair + 1) * LANES] = jnp.where(
            low, results[2 * pair], results[2 * pair + 1]
        ).astype(bf16)


def layer(
    sizes,
    x_hbm, context_hbm, condition, ctx_cond, gain, wsh_hbm, wsc_hbm, wga_hbm, wq_hbm, wk_hbm, wv_hbm, wo_hbm,
    sink_ref, lift_ref,
    out_hbm,
    x_v, context_v, wm_v, wq_v, wk_v, wv_v, wkv_v, wo_v,
    active_v, part_v, rx_v, zsrc_v, rz_v, mod_v, modr_v, mul_v, add_v,
    inv_v, cos_v, sin_v, qp_v, kv_v, ckv_v, kt_v, v4_v, att_v, by_v, out_v,
    local_sem, stage_sem, halo_send, halo_recv, wo_send, wo_recv, att_send, att_recv,
):
    nsp, nx, nt, nd = sizes
    nz = nsp // nx
    samples, tokens, width = x_v.shape
    chunk = tokens // nt
    ctx_local = context_v.shape[1]
    ctx = ctx_local * nsp
    sp = lax.axis_index("sp")
    tp = lax.axis_index("tp")
    dp = lax.axis_index("dp")
    xi = lax.rem(sp, nx)
    zi = lax.div(sp, nx)

    def place(sp_to=None, tp_to=None, dp_to=None):
        return {
            "sp": sp if sp_to is None else sp_to,
            "tp": tp if tp_to is None else tp_to,
            "dp": dp if dp_to is None else dp_to,
        }

    def remote(src, dst, send, recv, device):
        return pltpu.make_async_remote_copy(
            src_ref=src, dst_ref=dst, send_sem=send, recv_sem=recv, device_id=device, device_id_type=MESH
        )

    def x_peer(offset):
        return zi * nx + lax.rem(xi + offset, nx)

    def z_peer(offset):
        return lax.rem(zi + offset, nz) * nx + xi

    own_rows = wo_hbm.shape[0]
    half = own_rows // nd
    loads = [
        pltpu.make_async_copy(wsh_hbm, wm_v.at[0], local_sem.at[0]),
        pltpu.make_async_copy(wsc_hbm, wm_v.at[1], local_sem.at[1]),
        pltpu.make_async_copy(wga_hbm, wm_v.at[2], local_sem.at[2]),
        pltpu.make_async_copy(
            wo_hbm, wo_v.at[pl.ds(pl.multiple_of(tp * own_rows, own_rows), own_rows), :], local_sem.at[3]
        ),
        pltpu.make_async_copy(context_hbm, context_v, local_sem.at[4]),
        pltpu.make_async_copy(x_hbm, x_v, local_sem.at[5]),
        pltpu.make_async_copy(wk_hbm, wk_v, local_sem.at[6]),
        pltpu.make_async_copy(wv_hbm, wv_v, local_sem.at[7]),
        pltpu.make_async_copy(wq_hbm, wq_v, local_sem.at[8]),
    ]
    for load in loads:
        load.start()

    barrier = pltpu.get_barrier_semaphore()

    def greet(device):
        pl.semaphore_signal(barrier, inc=1, device_id=device, device_id_type=MESH)

    for offset in range(1, nsp):
        greet(place(sp_to=lax.rem(sp + offset, nsp)))
    for dy in range(1, nt):
        for dx in range(nx):
            greet(place(sp_to=x_peer(dx), tp_to=lax.rem(tp + dy, nt)))
    for offset in range(1, nd):
        greet(place(dp_to=lax.rem(dp + offset, nd)))

    active_v[...] = jnp.zeros_like(active_v)
    active_v[0:2, :] = condition[...].astype(f32)
    active_v[2:3, :] = ctx_cond[...].astype(f32)
    raw = active_v[...]
    active = (raw / (1.0 + jnp.exp(-raw))).astype(bf16)
    for load in loads[:3]:
        load.wait()
    vecs = [jnp.dot(active, wm_v[k], preferred_element_type=f32) for k in range(3)]
    for c in range(nx):
        cols = slice(c * LANES, (c + 1) * LANES)
        part_v[c, 0:3, :] = vecs[0][0:3, cols]
        part_v[c, 3:6, :] = vecs[1][0:3, cols]
        part_v[c, 6:8, :] = vecs[2][0:2, cols]

    pl.semaphore_wait(barrier, (nsp - 1) + (nt - 1) * nx + (nd - 1))

    for offset in range(1, nx):
        to = lax.rem(xi + offset, nx)
        remote(part_v.at[to], rx_v.at[offset - 1], stage_sem.at[0], stage_sem.at[1], place(sp_to=x_peer(offset))).start()

    loads[3].wait()

    def wo_rows(owner, core, start, count):
        return wo_v.at[pl.ds(pl.multiple_of(owner * own_rows + core * half + start, count), count), :]

    after = lax.rem(tp + 1, nt)
    before = lax.rem(tp + nt - 1, nt)
    across = lax.rem(tp + 2, nt)
    other = lax.rem(dp + 1, nd)
    quarter = half // 2

    def wo_copy(k, ref, device):
        return remote(ref, ref, wo_send.at[k], wo_recv.at[k], device)

    mine = wo_rows(tp, dp, 0, half)
    to_after = wo_copy(0, mine, place(tp_to=after))
    to_before = wo_copy(1, mine, place(tp_to=before))
    to_after.start()
    to_before.start()

    block = min(256, chunk)
    blocks = tokens // block

    def statistics(step):
        sample, start = step // blocks, pl.multiple_of(step % blocks * block, block)
        total = jnp.zeros((block, LANES), f32)
        for c in range(width // LANES):
            piece = x_v[sample, pl.ds(start, block), c * LANES : (c + 1) * LANES].astype(f32)
            total = total + piece * piece
        mean = jnp.sum(total, axis=1, keepdims=True) / width
        inv_v[sample, pl.ds(start, block), :] = jnp.broadcast_to(lax.rsqrt(mean + EPSILON), (block, LANES))

    low_wide = lanes_of(width) < HEAD
    loads[6].wait()
    loads[7].wait()
    wkv_v[...] = jnp.concatenate([wk_v[...], wv_v[...]], axis=1)
    loads[5].wait()

    def stats_loop(first, last):
        def run(step, carry):
            statistics(step)
            return carry

        lax.fori_loop(first, last, run, 0)

    all_blocks = samples * blocks
    stats_loop(0, all_blocks // 2)

    drain(rx_v, stage_sem.at[1])
    quarter_sum = part_v[xi]
    for k in range(nx - 1):
        quarter_sum = quarter_sum + rx_v[k]
    zsrc_v[...] = quarter_sum

    for offset in range(1, nz):
        remote(zsrc_v, rz_v.at[offset - 1], stage_sem.at[2], stage_sem.at[3], place(sp_to=z_peer(offset))).start()

    stats_loop(all_blocks // 2, all_blocks)
    lane1 = lanes_of(8)
    frequency = jnp.exp((lane1[0:1] % 16).astype(f32) * (-math.log(ROPE_BASE) / 16.0))
    grid_rows = tokens // GRID_COLS
    table_rows = max(grid_rows, 8)
    row_pos = (sp * grid_rows + lax.broadcasted_iota(jnp.int32, (table_rows, LANES), 0)).astype(f32)
    col_pos = lax.broadcasted_iota(jnp.int32, (GRID_COLS, LANES), 0).astype(f32)
    row_cos, row_sin = jnp.cos(row_pos * frequency), jnp.sin(row_pos * frequency)
    col_cos, col_sin = jnp.cos(col_pos * frequency), jnp.sin(col_pos * frequency)
    lane64 = lanes_of(GRID_COLS)
    by_row = lane64 % HEAD < 32
    minus = lane64 % 32 < 16
    for t in range(grid_rows):
        rows = slice(t * GRID_COLS, (t + 1) * GRID_COLS)
        cos_v[rows, :] = jnp.where(by_row, row_cos[t : t + 1, :], col_cos)
        sine = jnp.where(by_row, row_sin[t : t + 1, :], col_sin)
        sin_v[rows, :] = jnp.where(minus, -sine, sine)

    drain(rz_v, stage_sem.at[3])
    total = zsrc_v[...]
    for k in range(nz - 1):
        total = total + rz_v[k]
    here = tp * nx + xi
    mod_v[here] = total

    for dy in range(nt):
        for dx in range(nx):
            if dy or dx:
                remote(
                    mod_v.at[here], mod_v.at[here], stage_sem.at[4], stage_sem.at[5],
                    place(sp_to=x_peer(dx), tp_to=lax.rem(tp + dy, nt)),
                ).start()

    @pl.when(sp == 0)
    def _():
        kv_v[:, 0:WINDOW, :] = jnp.zeros((samples, WINDOW, LANES), bf16)

    @pl.when(sp == nsp - 1)
    def _():
        kv_v[:, WINDOW + tokens :, :] = jnp.zeros((samples, WINDOW, LANES), bf16)

    loads[4].wait()
    loads[8].wait()
    ctx_rows = samples * ctx_local
    ctx_wide = context_v[...].reshape(ctx_rows, width).astype(f32)
    ctx_inv = lax.rsqrt(jnp.mean(ctx_wide * ctx_wide, axis=1, keepdims=True) + EPSILON)
    ctx_unit = ctx_wide * ctx_inv

    drain(mod_v.at[pl.ds(0, nt * nx - 1)], stage_sem.at[5])
    for k in range(nt * nx):
        modr_v[:, k * LANES : (k + 1) * LANES] = mod_v[k]
    scaled = gain[...] * (1.0 + modr_v[3:6, :])
    for r in range(samples):
        mul_v[r, 0:1, :] = scaled[r : r + 1]
        add_v[r, 0:1, :] = modr_v[r : r + 1, :]

    ctx_hidden = (ctx_unit * scaled[2:3] + modr_v[2:3, :]).astype(bf16)
    ctx_pairs = jnp.dot(ctx_hidden, wkv_v[...], preferred_element_type=f32).astype(bf16)
    ckv_v[sp] = ctx_pairs.reshape(samples, ctx_local, LANES)
    for offset in range(1, nsp):
        remote(
            ckv_v.at[sp], ckv_v.at[sp], stage_sem.at[6], stage_sem.at[7], place(sp_to=lax.rem(sp + offset, nsp))
        ).start()

    from_before = wo_rows(before, dp, 0, half)
    from_after = wo_rows(after, dp, 0, half)
    wo_copy(0, from_before, place(tp_to=after)).wait_recv()
    on_after = wo_copy(2, wo_rows(before, dp, 0, quarter), place(tp_to=after))
    on_after.start()
    wo_copy(1, from_after, place(tp_to=before)).wait_recv()
    on_before = wo_copy(3, wo_rows(after, dp, quarter, quarter), place(tp_to=before))
    on_before.start()
    over_before = wo_copy(4, from_before, place(dp_to=other))
    over_after = wo_copy(5, from_after, place(dp_to=other))
    over_before.start()
    over_after.start()

    lane = lanes_of(block)
    low = lane < HEAD

    def project(sample, index):
        start = pl.multiple_of(index * block, block)
        inverse = inv_v[sample, pl.ds(start, block), :]
        steps = 4
        deep = width // steps
        q_acc = jnp.zeros((block, 2 * LANES), f32)
        kv_acc = jnp.zeros((block, LANES), f32)
        for k in range(steps):
            pieces = []
            for c in range(deep // LANES):
                cols = slice(k * deep + c * LANES, k * deep + (c + 1) * LANES)
                wide = x_v[sample, pl.ds(start, block), cols].astype(f32)
                pieces.append(
                    (wide * inverse * mul_v[sample, 0:1, cols] + add_v[sample, 0:1, cols]).astype(bf16)
                )
            hidden = jnp.concatenate(pieces, axis=1)
            q_acc = q_acc + jnp.dot(hidden, wq_v[k * deep : (k + 1) * deep, :], preferred_element_type=f32)
            kv_acc = kv_acc + jnp.dot(hidden, wkv_v[k * deep : (k + 1) * deep, :], preferred_element_type=f32)
        cosine = cos_v[pl.ds(start, block), :]
        sine = sin_v[pl.ds(start, block), :]
        turned = kv_acc * cosine + swapped(kv_acc, lane) * sine
        kv_v[sample, pl.ds(pl.multiple_of(WINDOW + start, WINDOW), block), :] = jnp.where(low, turned, kv_acc).astype(bf16)
        factor = HEAD ** (-0.5) * LOG2E
        for pair in range(2):
            u = q_acc[:, pair * LANES : (pair + 1) * LANES]
            turned = (u * cosine + swapped(u, lane) * sine) * factor
            qp_v[sample, 2 * pair, pl.ds(start, block), :] = jnp.where(low, turned, 0.0).astype(bf16)
            qp_v[sample, 2 * pair + 1, pl.ds(start, block), :] = jnp.where(low, 0.0, turned).astype(bf16)

    def edges(step, carry):
        project(step // 2, step % 2 * (blocks - 1))
        return carry

    lax.fori_loop(0, 2 * samples, edges, 0)

    send_right = remote(
        kv_v.at[:, pl.ds(tokens, WINDOW), :], kv_v.at[:, pl.ds(0, WINDOW), :], halo_send.at[0], halo_recv.at[0],
        place(sp_to=lax.rem(sp + 1, nsp)),
    )
    send_left = remote(
        kv_v.at[:, pl.ds(WINDOW, WINDOW), :], kv_v.at[:, pl.ds(WINDOW + tokens, WINDOW), :], halo_send.at[1],
        halo_recv.at[1], place(sp_to=lax.rem(sp + nsp - 1, nsp)),
    )

    @pl.when(sp < nsp - 1)
    def _():
        send_right.start()

    @pl.when(sp > 0)
    def _():
        send_left.start()

    inner = blocks - 2

    def middles(step, carry):
        project(step // inner, 1 + step % inner)
        return carry

    lax.fori_loop(0, inner * samples, middles, 0)

    from_across = wo_rows(across, dp, 0, half)
    wo_copy(2, wo_rows(across, dp, 0, quarter), place(tp_to=after)).wait_recv()
    wo_copy(3, wo_rows(across, dp, quarter, quarter), place(tp_to=before)).wait_recv()
    over_across = wo_copy(6, from_across, place(dp_to=other))
    over_across.start()

    @pl.when(sp > 0)
    def _():
        send_right.wait_recv()

    @pl.when(sp < nsp - 1)
    def _():
        send_left.wait_recv()

    for sample in range(samples):
        prepare(kv_v[sample], kt_v, v4_v, sample, ctx, tokens + 2 * WINDOW)
    drain(ckv_v.at[pl.ds(0, nsp - 1)], stage_sem.at[7])
    for sample in range(samples):
        prepare(ckv_v[:, sample].reshape(ctx, LANES), kt_v, v4_v, sample, 0, ctx)

    def att_copy(step_k, sample, dest):
        return remote(
            att_v.at[sample, pl.ds(pl.multiple_of(dest * chunk, chunk), chunk), :], by_v.at[tp, sample],
            att_send.at[step_k, sample], att_recv.at[step_k, sample], place(tp_to=dest),
        )

    def chunk_step(step, carry):
        k, sample = step // samples, step % samples
        dest = lax.rem(tp + 1 + k, nt)
        for sub in range(chunk // WINDOW):
            row = pl.multiple_of(dest * chunk + sub * WINDOW, WINDOW)
            left_off = jnp.where((sp == 0) & (row == 0), NEGATIVE, 0.0)
            right_off = jnp.where((sp == nsp - 1) & (row == tokens - WINDOW), NEGATIVE, 0.0)
            attend(
                sample, row, pl.multiple_of(ctx + row, WINDOW), left_off, right_off, qp_v, kt_v, v4_v, lift_ref,
                sink_ref, att_v, ctx,
            )

        @pl.when(k < nt - 1)
        def _():
            att_copy(k, sample, dest).start()

        return carry

    lax.fori_loop(0, nt * samples, chunk_step, 0)
    by_v[tp] = att_v[:, pl.ds(pl.multiple_of(tp * chunk, chunk), chunk), :]

    for k in (4, 5, 6):
        wo_copy(k, wo_rows(tp, dp, 0, half), place(dp_to=other)).wait_recv()
    for k in range(nt - 1):
        for sample in range(samples):
            att_copy(k, sample, lax.rem(tp + 1 + k, nt)).wait_recv()

    wide = 512
    for sample in range(samples):

        def project_out(step, carry):
            cols = pl.ds(pl.multiple_of(step * wide, wide), wide)
            total = jnp.zeros((chunk, wide), f32)
            for t in range(nt):
                total = total + jnp.dot(
                    by_v[t, sample], wo_v[t * own_rows : (t + 1) * own_rows, cols], preferred_element_type=f32
                )
            out_v[sample, :, cols] = (total * modr_v[6 + sample : 7 + sample, cols]).astype(bf16)
            return carry

        lax.fori_loop(0, width // wide, project_out, 0)
        pltpu.make_async_copy(out_v.at[sample], out_hbm.at[sample], local_sem.at[9 + sample]).start()

    drain(rx_v, stage_sem.at[0])
    drain(rz_v, stage_sem.at[2])
    drain(mod_v.at[pl.ds(0, nt * nx - 1)], stage_sem.at[4])
    drain(ckv_v.at[pl.ds(0, nsp - 1)], stage_sem.at[6])
    for copy in (to_after, to_before, on_after, on_before, over_before, over_after, over_across):
        copy.wait_send()

    @pl.when(sp < nsp - 1)
    def _():
        send_right.wait_send()

    @pl.when(sp > 0)
    def _():
        send_left.wait_send()

    for k in range(nt - 1):
        for sample in range(samples):
            att_copy(k, sample, lax.rem(tp + 1 + k, nt)).wait_send()
    for sample in range(samples):
        pltpu.make_async_copy(out_v.at[sample], out_hbm.at[sample], local_sem.at[9 + sample]).wait()


def shards(
    sizes, latent, context, condition, ctx_cond, norm_gain, w_shift, w_scale, w_gate, w_query, w_key, w_value, w_out,
    sink_logit, ctx_lift,
):
    nsp, nx, nt, nd = sizes
    nz = nsp // nx
    samples, tokens, width = latent.shape
    ctx_local = context.shape[1]
    ctx = ctx_local * nsp
    feats = condition.shape[1]
    cols = w_shift.shape[1]
    chunk = tokens // nt
    keys = ctx + tokens + 2 * WINDOW
    own_rows = w_out.shape[0]
    anywhere = pl.BlockSpec(memory_space=pl.ANY)
    vmem = pl.BlockSpec(memory_space=pltpu.VMEM)
    smem = pl.BlockSpec(memory_space=pltpu.SMEM)
    dma = pltpu.SemaphoreType.DMA
    return pl.pallas_call(
        functools.partial(layer, sizes),
        out_shape=jax.ShapeDtypeStruct((samples, chunk, width), bf16),
        in_specs=[anywhere, anywhere, vmem, vmem, vmem] + [anywhere] * 7 + [smem, smem],
        out_specs=anywhere,
        scratch_shapes=[
            pltpu.VMEM((samples, tokens, width), bf16),
            pltpu.VMEM((samples, ctx_local, width), bf16),
            pltpu.VMEM((3, feats, cols), bf16),
            pltpu.VMEM((width, 4 * HEAD), bf16),
            pltpu.VMEM((width, HEAD), bf16),
            pltpu.VMEM((width, HEAD), bf16),
            pltpu.VMEM((width, LANES), bf16),
            pltpu.VMEM((own_rows * nt, width), bf16),
            pltpu.VMEM((16, feats), f32),
            pltpu.VMEM((nx, 8, LANES), f32),
            pltpu.VMEM((nx - 1, 8, LANES), f32),
            pltpu.VMEM((8, LANES), f32),
            pltpu.VMEM((nz - 1, 8, LANES), f32),
            pltpu.VMEM((nt * nx, 8, LANES), f32),
            pltpu.VMEM((8, width), f32),
            pltpu.VMEM((samples, 8, width), f32),
            pltpu.VMEM((samples, 8, width), f32),
            pltpu.VMEM((samples, tokens, LANES), f32),
            pltpu.VMEM((tokens, LANES), f32),
            pltpu.VMEM((tokens, LANES), f32),
            pltpu.VMEM((samples, 4, tokens, LANES), bf16),
            pltpu.VMEM((samples, tokens + 2 * WINDOW, LANES), bf16),
            pltpu.VMEM((nsp, samples, ctx_local, LANES), bf16),
            pltpu.VMEM((samples, LANES, keys), bf16),
            pltpu.VMEM((samples, keys, 2 * LANES), bf16),
            pltpu.VMEM((samples, tokens, 2 * LANES), bf16),
            pltpu.VMEM((nt, samples, chunk, 2 * LANES), bf16),
            pltpu.VMEM((samples, chunk, width), bf16),
            dma((9 + samples,)),
            dma((8,)),
            dma((2,)),
            dma((2,)),
            dma((7,)),
            dma((7,)),
            dma((nt - 1, samples)),
            dma((nt - 1, samples)),
        ],
        compiler_params=pltpu.CompilerParams(
            collective_id=0, has_side_effects=True, vmem_limit_bytes=62 * 1024 * 1024
        ),
        name="layer",
    )(
        latent, context, condition, ctx_cond.reshape(1, feats), norm_gain.reshape(1, width), w_shift, w_scale, w_gate,
        w_query, w_key, w_value, w_out, sink_logit, ctx_lift,
    )


def solution(mesh):
    nsp, nt, nd = mesh.shape["sp"], mesh.shape["tp"], mesh.shape["dp"]
    sizes = (nsp, 4 if nsp > 4 else 2, nt, nd)
    return jax.shard_map(
        functools.partial(shards, sizes),
        mesh=mesh,
        in_specs=(
            P("dp", "sp", None),
            P("dp", "sp", None),
            P("dp", "sp"),
            P("sp"),
            P(),
            P("sp", "tp"),
            P("sp", "tp"),
            P("sp", "tp"),
            P(None, "tp"),
            P(None, "tp"),
            P(None, "tp"),
            P("tp", None),
            P("tp"),
            P("tp"),
        ),
        out_specs=P("dp", ("sp", "tp"), None),
        check_vma=False,
    )
```

time: 221 us -> 72.1 us (0.33); the launches traced: 216 us -> 70.9 us
  matrix products: 71.6 us -> 0 us
  Pallas kernels: 0 us -> 63.8 us
  other arithmetic: 39.5 us -> 0 us
  blocking collectives: 28.1 us -> 0 us
  starting transfers between devices: 24 us -> 0 us
  between operations: 13.7 us -> 0.01 us
  waiting for transfers between devices: 13.1 us -> 0 us
  loops' own time: 10.8 us -> 0 us
  local copies, waits for them, and re-layouts: 15.7 us -> 7.07 us
    dot_general x25 -> x0, matrix products: 71.6 us -> none  [the longest x4 18.2 us: attend(): jnp.einsum('qgrd,kgd->grqk', q_rows, far_keys, preferred_element_type=jnp...]
    pallas_call x0 -> x1, Pallas kernels: none -> 63.8 us  [shards(): pl.pallas_call(functools.partial(layer, sizes), out_shape=jax.ShapeDtypeS...]
    reduce_sum x11 -> x0, other arithmetic: 33 us -> none  [the longest x4 21 us: attend(): far_exp.sum(-1, keepdims=True)]
    all_to_all x2 -> x0, starting transfers between devices: 16 us -> none  [copy_for_each(): return lax.all_to_all(copies, axis, split_axis=0, concat_axis=0, tiled=True)]
    all_to_all x1 -> x0, blocking collectives: 14.6 us -> none  [shards(): lax.all_to_all(attended, 'tp', split_axis=1, concat_axis=2, tiled=True)]
    all_gather x1 -> x0, blocking collectives: 13.5 us -> none  [sent_together(): whole = lax.all_gather(both, axis, axis=dim, tiled=True)]
    all_to_all x2 -> x0, waiting for transfers between devices: 11 us -> none  [copy_for_each(): return lax.all_to_all(copies, axis, split_axis=0, concat_axis=0, tiled=True)]
    another operation x1 -> x0, loops' own time: 10.8 us -> none  [shards(): lax.map(attend, jnp.arange(samples * blocks, dtype=jnp.int32))]
  transfers between devices with their start and end apart: 5 -> 0, of which waited for: 2 -> 0; matrix products, arithmetic and copies ran while one was open for 54% -> 0% of each run, Pallas kernels for 0% -> 0%
where the time goes in v1:
time: 72.1 us; the launch traced here: 70.9 us
  Pallas kernels  63.8 us (88%)
  local copies, waits for them, and re-layouts  7.07 us (10%)
    pallas_call x1, Pallas kernels, shards(): pl.pallas_call(functools.partial(layer, sizes), out_shape=jax.ShapeDtypeS...  63.8 us
    unnamed x3, local copies, waits for them, and re-layouts  7.07 us

profile of v1, /device:TPU:32, one launch (start us, length us, event | category | flops | bytes accessed | tf_op | source)
XLA Modules:
  0.0 70.9 jit_solution(4267981023158976699)
XLA Ops:
  0.0 2.0 %copy.15.wk_hbm = bf16[2048,64]{1,0:T(8,128)(2,1)} copy(bf16[2048,64]{0,1:T(8,128)(2,1)} %param.23) | data formatting | bytes 524288 | tf_op args[9]
  2.0 2.0 %copy.16.wv_hbm = bf16[2048,64]{1,0:T(8,128)(2,1)} copy(bf16[2048,64]{0,1:T(8,128)(2,1)} %param.24) | data formatting | bytes 524288 | tf_op args[10]
  3.9 63.8 %layer.1 = bf16[2,256,2048]{2,1,0:T(8,128)(2,1)} custom-call(bf16[2,1024,2048]{2,1,0:T(8,128)(2,1)} %x_hbm.1, bf16[2,32,2048]{2,1,0:T(8,128)(2,1)} %context_hbm.1, bf16[2,64]{1,0:T(2,128)(2,1)} %condition.1, bf16[1,64]{1,0:T(2,128)(2,1)} %bitcast.3, f32[1,2048]{1,0:T(1,128)} %bitcast.2, bf16[64,512]{1,0:T(8,128)(2,1)} %wsh_hbm.1, bf16[64,512]{1,0:T(8,128)(2,1)} %wsc_hbm.1, ...), custom_call_target="tpu_custom_call" | custom-call | tf_op jit(solution)/shard_map/layer/pallas_call | solution.py:480
  67.7 3.2 %copy.18 = bf16[2,256,2048]{2,1,0:T(8,128)(2,1)} copy(bf16[2,256,2048]{2,1,0:T(8,128)(2,1)} %layer.1) | data formatting | bytes 4194304

commit v2 on v1

v2 whole, which is shorter than its diff:
```python
import functools
import math

import jax
import jax.numpy as jnp
from jax import lax
from jax.experimental import pallas as pl
from jax.experimental.pallas import tpu as pltpu
from jax.sharding import PartitionSpec as P

HEAD = 64
WINDOW = 128
GRID_COLS = 64
EPSILON = 1e-06
ROPE_BASE = 10000.0
NEGATIVE = -1e30
LOG2E = math.log2(math.e)
LANES = 128
MESH = pl.DeviceIdType.MESH
f32 = jnp.float32
bf16 = jnp.bfloat16


def lanes_of(rows):
    return lax.broadcasted_iota(jnp.int32, (rows, LANES), 1)


def drain(ref, sem):
    pltpu.make_async_copy(ref, ref, sem).wait()


def swapped(u, lane):
    return jnp.where(lane % 32 < 16, pltpu.roll(u, LANES - 16, 1), pltpu.roll(u, 16, 1))


class Scores:
    def __init__(self, refs, sample, row, left_off, right_off, score_ref, top_ref):
        self.kv, self.ckv, q_ref, self.limits = refs
        self.sample, self.row, self.offsets = sample, row, {0: left_off, 2 * WINDOW: right_off}
        self.score_ref, self.top_ref = score_ref, top_ref
        turned = q_ref[sample, pl.ds(row, WINDOW), :].astype(f32).T.astype(bf16)
        self.q = jnp.concatenate([turned[h * HEAD : (h + 1) * HEAD] for h in range(4)], axis=1)
        self.tops = {}

    def piece(self, kind, at, put, rows):
        ctx_local = self.ckv.shape[2]
        if kind == "far":
            keys = self.ckv[self.sample, at // ctx_local : (at + rows) // ctx_local].reshape(rows, LANES)
        else:
            keys = self.kv[self.sample, pl.ds(pl.multiple_of(self.row + at, WINDOW), rows), :]
        score = jnp.dot(keys[:, :HEAD], self.q, preferred_element_type=f32)
        if kind == "near" and at != WINDOW:
            key = lax.broadcasted_iota(jnp.int32, score.shape, 0)
            query = lax.broadcasted_iota(jnp.int32, score.shape, 1) % WINDOW
            inside = key >= query if at == 0 else key <= query
            score = jnp.where(inside, score, NEGATIVE) + self.offsets[at]
        self.score_ref[put : put + rows, :] = score
        top = jnp.max(score.reshape(rows // 8, 8, score.shape[1]), axis=0)
        self.tops[kind] = jnp.maximum(self.tops[kind], top) if kind in self.tops else top

    def done(self):
        far = jnp.max(self.tops["far"], axis=0, keepdims=True) + self.limits[0:1, :]
        near = jnp.max(self.tops["near"], axis=0, keepdims=True)
        self.top_ref[0:1, :] = jnp.maximum(jnp.maximum(far, near), self.limits[1:2, :])


class Weights:
    def __init__(self, vt, limits, att, ctx, sample, row, score_ref, top_ref):
        self.vt, self.att, self.ctx, self.sample, self.row, self.score_ref = vt, att, ctx, sample, row, score_ref
        self.top = top_ref[0:1, :]
        self.lowered = self.top - limits[0:1, :]
        self.sink = jnp.exp2(limits[1:2, :] - self.top)
        self.total = jnp.zeros((vt.shape[1], 4 * WINDOW), f32)

    def piece(self, kind, at, put, rows):
        top = self.lowered if kind == "far" else self.top
        weight = jnp.exp2(self.score_ref[put : put + rows, :] - top).astype(bf16)
        if kind == "far":
            values = self.vt[self.sample, :, at : at + rows]
        else:
            values = self.vt[self.sample, :, pl.ds(pl.multiple_of(self.ctx + self.row + at, WINDOW), rows)]
        self.total = self.total + jnp.dot(values, weight, preferred_element_type=f32)

    def done(self):
        out = self.total[16:] * (1.0 / (self.total[0:1] + self.sink))
        stacked = jnp.concatenate([out[:, h * WINDOW : (h + 1) * WINDOW] for h in range(4)], axis=0)
        self.att[self.sample, pl.ds(self.row, WINDOW), :] = stacked.T.astype(bf16)


def layer(
    sizes,
    x_hbm, context_hbm, condition, ctx_cond, gain, wsh_hbm, wsc_hbm, wga_hbm, wq_hbm, wk_hbm, wv_hbm, wo_hbm,
    sink_ref, lift_ref,
    out_v,
    x_v, context_v, wm_v, wq_v, wt_v, wkv_v, wo_v,
    active_v, part_v, rx_v, zsrc_v, rz_v, mod_v, modr_v, mul_v, add_v,
    inv_v, cos_v, sin_v, q_v, kv_v, ckv_v, vt_v, limits_v, s0_v, s1_v, t0_v, t1_v, att_v, by_v,
    local_sem, stage_sem, ctx_sem, halo_send, halo_recv, wo_send, wo_recv, att_send, att_recv,
):
    nsp, nx, nt, nd = sizes
    nz = nsp // nx
    samples, tokens, width = x_v.shape
    chunk = tokens // nt
    ctx_local = context_v.shape[1]
    ctx = ctx_local * nsp
    sp = lax.axis_index("sp")
    tp = lax.axis_index("tp")
    dp = lax.axis_index("dp")
    xi = lax.rem(sp, nx)
    zi = lax.div(sp, nx)

    def place(sp_to=None, tp_to=None, dp_to=None):
        return {
            "sp": sp if sp_to is None else sp_to,
            "tp": tp if tp_to is None else tp_to,
            "dp": dp if dp_to is None else dp_to,
        }

    def remote(src, dst, send, recv, device):
        return pltpu.make_async_remote_copy(
            src_ref=src, dst_ref=dst, send_sem=send, recv_sem=recv, device_id=device, device_id_type=MESH
        )

    def x_peer(offset):
        return zi * nx + lax.rem(xi + offset, nx)

    def z_peer(offset):
        return lax.rem(zi + offset, nz) * nx + xi

    own_rows = wo_hbm.shape[0]
    half = own_rows // nd
    loads = [
        pltpu.make_async_copy(wsh_hbm, wm_v.at[0], local_sem.at[0]),
        pltpu.make_async_copy(wsc_hbm, wm_v.at[1], local_sem.at[1]),
        pltpu.make_async_copy(wga_hbm, wm_v.at[2], local_sem.at[2]),
        pltpu.make_async_copy(
            wo_hbm, wo_v.at[pl.ds(pl.multiple_of(tp * own_rows, own_rows), own_rows), :], local_sem.at[3]
        ),
        pltpu.make_async_copy(context_hbm, context_v, local_sem.at[4]),
        pltpu.make_async_copy(x_hbm, x_v, local_sem.at[5]),
        pltpu.make_async_copy(wk_hbm, wt_v.at[pl.ds(0, HEAD), :], local_sem.at[6]),
        pltpu.make_async_copy(wv_hbm, wt_v.at[pl.ds(HEAD, HEAD), :], local_sem.at[7]),
        pltpu.make_async_copy(wq_hbm, wq_v, local_sem.at[8]),
    ]
    for load in loads:
        load.start()

    barrier = pltpu.get_barrier_semaphore()

    def greet(device):
        pl.semaphore_signal(barrier, inc=1, device_id=device, device_id_type=MESH)

    for offset in range(1, nx):
        greet(place(sp_to=x_peer(offset)))
    for offset in range(1, nz):
        greet(place(sp_to=z_peer(offset)))
    for offset in range(1, nt):
        greet(place(tp_to=lax.rem(tp + offset, nt)))
    for offset in range(1, nd):
        greet(place(dp_to=lax.rem(dp + offset, nd)))

    active_v[...] = jnp.zeros_like(active_v)
    active_v[0:2, :] = condition[...].astype(f32)
    active_v[2:3, :] = ctx_cond[...].astype(f32)
    raw = active_v[...]
    active = (raw / (1.0 + jnp.exp(-raw))).astype(bf16)
    for load in loads[:3]:
        load.wait()
    vecs = [jnp.dot(active, wm_v[k], preferred_element_type=f32) for k in range(3)]
    for c in range(nx):
        cols = slice(c * LANES, (c + 1) * LANES)
        part_v[c, 0:3, :] = vecs[0][0:3, cols]
        part_v[c, 3:6, :] = vecs[1][0:3, cols]
        part_v[c, 6:8, :] = vecs[2][0:2, cols]

    pl.semaphore_wait(barrier, (nx - 1) + (nz - 1) + (nt - 1) + (nd - 1))

    for offset in range(1, nx):
        to = lax.rem(xi + offset, nx)
        remote(part_v.at[to], rx_v.at[offset - 1], stage_sem.at[0], stage_sem.at[1], place(sp_to=x_peer(offset))).start()

    loads[3].wait()

    def wo_rows(owner, core, start, count):
        return wo_v.at[pl.ds(pl.multiple_of(owner * own_rows + core * half + start, count), count), :]

    after = lax.rem(tp + 1, nt)
    before = lax.rem(tp + nt - 1, nt)
    across = lax.rem(tp + 2, nt)
    other = lax.rem(dp + 1, nd)
    quarter = half // 2

    def wo_copy(k, ref, device):
        return remote(ref, ref, wo_send.at[k], wo_recv.at[k], device)

    wo_sends = [
        wo_copy(0, wo_rows(tp, dp, 0, quarter), place(tp_to=after)),
        wo_copy(1, wo_rows(tp, dp, 0, quarter), place(tp_to=before)),
        wo_copy(2, wo_rows(tp, dp, quarter, quarter), place(tp_to=after)),
        wo_copy(3, wo_rows(tp, dp, quarter, quarter), place(tp_to=before)),
        wo_copy(4, wo_rows(before, dp, 0, quarter), place(tp_to=after)),
        wo_copy(5, wo_rows(after, dp, quarter, quarter), place(tp_to=before)),
        wo_copy(6, wo_rows(before, dp, 0, half), place(dp_to=other)),
        wo_copy(7, wo_rows(after, dp, 0, half), place(dp_to=other)),
        wo_copy(8, wo_rows(across, dp, 0, half), place(dp_to=other)),
    ]
    wo_sends[0].start()
    wo_sends[1].start()

    block = min(256, chunk)
    blocks = tokens // block

    def statistics(step):
        sample, start = step // blocks, pl.multiple_of(step % blocks * block, block)
        total = jnp.zeros((block, LANES), f32)
        for c in range(width // LANES):
            piece = x_v[sample, pl.ds(start, block), c * LANES : (c + 1) * LANES].astype(f32)
            total = total + piece * piece
        mean = jnp.sum(total, axis=1, keepdims=True) / width
        inv_v[sample, pl.ds(start, block), :] = jnp.broadcast_to(lax.rsqrt(mean + EPSILON), (block, LANES))

    loads[6].wait()
    loads[7].wait()
    wkv_v[...] = wt_v[...].T
    loads[5].wait()

    def stats_loop(first, last):
        def run(step, carry):
            statistics(step)
            return carry

        lax.fori_loop(first, last, run, 0)

    all_blocks = samples * blocks
    stats_loop(0, all_blocks // 2)

    drain(rx_v, stage_sem.at[1])
    quarter_sum = part_v[xi]
    for k in range(nx - 1):
        quarter_sum = quarter_sum + rx_v[k]
    zsrc_v[...] = quarter_sum

    for offset in range(1, nz):
        remote(zsrc_v, rz_v.at[offset - 1], stage_sem.at[2], stage_sem.at[3], place(sp_to=z_peer(offset))).start()

    stats_loop(all_blocks // 2, all_blocks)
    lane1 = lanes_of(8)
    frequency = jnp.exp((lane1[0:1] % 16).astype(f32) * (-math.log(ROPE_BASE) / 16.0))
    grid_rows = tokens // GRID_COLS
    table_rows = max(grid_rows, 8)
    row_pos = (sp * grid_rows + lax.broadcasted_iota(jnp.int32, (table_rows, LANES), 0)).astype(f32)
    col_pos = lax.broadcasted_iota(jnp.int32, (GRID_COLS, LANES), 0).astype(f32)
    row_cos, row_sin = jnp.cos(row_pos * frequency), jnp.sin(row_pos * frequency)
    col_cos, col_sin = jnp.cos(col_pos * frequency), jnp.sin(col_pos * frequency)
    lane64 = lanes_of(GRID_COLS)
    by_row = lane64 % HEAD < 32
    minus = lane64 % 32 < 16
    for t in range(grid_rows):
        rows = slice(t * GRID_COLS, (t + 1) * GRID_COLS)
        cos_v[rows, :] = jnp.where(by_row, row_cos[t : t + 1, :], col_cos)
        sine = jnp.where(by_row, row_sin[t : t + 1, :], col_sin)
        sin_v[rows, :] = jnp.where(minus, -sine, sine)

    drain(rz_v, stage_sem.at[3])
    total = zsrc_v[...]
    for k in range(nz - 1):
        total = total + rz_v[k]
    here = tp * nx + xi
    mod_v[here] = total

    for dy in range(nt):
        for dx in range(nx):
            if dy or dx:
                remote(
                    mod_v.at[here], mod_v.at[here], stage_sem.at[4], stage_sem.at[5],
                    place(sp_to=x_peer(dx), tp_to=lax.rem(tp + dy, nt)),
                ).start()

    wo_sends[0].wait_recv()
    wo_sends[4].start()
    wo_sends[2].start()
    wo_sends[3].start()

    @pl.when(sp == 0)
    def _():
        kv_v[:, 0:WINDOW, :] = jnp.zeros((samples, WINDOW, LANES), bf16)

    @pl.when(sp == nsp - 1)
    def _():
        kv_v[:, WINDOW + tokens :, :] = jnp.zeros((samples, WINDOW, LANES), bf16)

    loads[4].wait()
    loads[8].wait()
    ctx_rows = samples * ctx_local
    ctx_wide = context_v[...].reshape(ctx_rows, width).astype(f32)
    ctx_inv = lax.rsqrt(jnp.mean(ctx_wide * ctx_wide, axis=1, keepdims=True) + EPSILON)
    ctx_unit = ctx_wide * ctx_inv

    drain(mod_v.at[pl.ds(0, nt * nx - 1)], stage_sem.at[5])
    for k in range(nt * nx):
        modr_v[:, k * LANES : (k + 1) * LANES] = mod_v[k]
    scaled = gain[...] * (1.0 + modr_v[3:6, :])
    for r in range(samples):
        mul_v[r, 0:1, :] = scaled[r : r + 1]
        add_v[r, 0:1, :] = modr_v[r : r + 1, :]

    ctx_hidden = (ctx_unit * scaled[2:3] + modr_v[2:3, :]).astype(bf16)
    ctx_pairs = jnp.dot(ctx_hidden, wkv_v[...], preferred_element_type=f32).astype(bf16)
    ckv_v[:, pl.ds(sp, 1)] = ctx_pairs.reshape(samples, 1, ctx_local, LANES)

    def ctx_rows_of(owner):
        return ckv_v.at[:, pl.ds(owner, 1)]

    def ctx_along_x(owner_z):
        rows = ctx_rows_of(owner_z * nx + xi)
        for offset in range(1, nx):
            remote(rows, rows, stage_sem.at[6], stage_sem.at[7], place(sp_to=x_peer(offset))).start()

    def ctx_along_z(offset):
        rows = ctx_rows_of(sp)
        return remote(rows, rows, ctx_sem.at[0, offset], ctx_sem.at[1, offset], place(sp_to=z_peer(offset)))

    for offset in range(1, nz):
        ctx_along_z(offset).start()
    ctx_along_x(zi)

    def pass_on(offsets):
        for offset in offsets:
            ctx_along_z(offset).wait_recv()
            ctx_along_x(lax.rem(zi + nz - offset, nz))

    far_z = [offset for offset in range(1, nz) if 2 < offset < nz - 2]
    near_z = [offset for offset in range(1, nz) if offset not in far_z]

    lane = lanes_of(block)
    low = lane < HEAD

    assert blocks == 4 and samples == 2
    steps = 4
    deep = width // steps
    factor = HEAD ** (-0.5) * LOG2E

    def block_of(step):
        late, turn = step // 4, step % 4
        index = (1 - late) * (turn % 2) * (blocks - 1) + late * (1 + turn % 2)
        return turn // 2, pl.multiple_of(index * block, block)

    def store_values(pairs_t, sample, start):
        vt_v[sample, 16:, pl.ds(start, pairs_t.shape[1])] = pairs_t[HEAD:].astype(bf16)

    def project(step):
        sample, start = block_of(step)
        inverse = inv_v[sample, pl.ds(start, block), :]
        q_acc = jnp.zeros((block, 2 * LANES), f32)
        kv_acc = jnp.zeros((block, LANES), f32)
        for k in range(steps):
            hidden = []
            for c in range(deep // LANES):
                cols = slice(k * deep + c * LANES, k * deep + (c + 1) * LANES)
                wide = x_v[sample, pl.ds(start, block), cols].astype(f32)
                hidden.append((wide * inverse * mul_v[sample, 0:1, cols] + add_v[sample, 0:1, cols]).astype(bf16))
            hidden = jnp.concatenate(hidden, axis=1)
            q_acc = q_acc + jnp.dot(hidden, wq_v[k * deep : (k + 1) * deep, :], preferred_element_type=f32)
            kv_acc = kv_acc + jnp.dot(hidden, wkv_v[k * deep : (k + 1) * deep, :], preferred_element_type=f32)
        cosine = cos_v[pl.ds(start, block), :]
        sine = sin_v[pl.ds(start, block), :]
        turned = jnp.where(low, kv_acc * cosine + swapped(kv_acc, lane) * sine, kv_acc)
        kv_v[sample, pl.ds(pl.multiple_of(WINDOW + start, WINDOW), block), :] = turned.astype(bf16)
        store_values(turned.T, sample, pl.multiple_of(ctx + WINDOW + start, WINDOW))
        for pair in range(2):
            u = q_acc[:, pair * LANES : (pair + 1) * LANES]
            turned = (u * cosine + swapped(u, lane) * sine) * factor
            q_v[sample, pl.ds(start, block), pair * LANES : (pair + 1) * LANES] = turned.astype(bf16)

    send_right = remote(
        kv_v.at[:, pl.ds(tokens, WINDOW), :], kv_v.at[:, pl.ds(0, WINDOW), :], halo_send.at[0], halo_recv.at[0],
        place(sp_to=lax.rem(sp + 1, nsp)),
    )
    send_left = remote(
        kv_v.at[:, pl.ds(WINDOW, WINDOW), :], kv_v.at[:, pl.ds(WINDOW + tokens, WINDOW), :], halo_send.at[1],
        halo_recv.at[1], place(sp_to=lax.rem(sp + nsp - 1, nsp)),
    )

    def project_group(group, carry):
        for member in range(4):
            project(4 * group + member)

        @pl.when((group == 0) & (sp < nsp - 1))
        def _():
            send_right.start()

        @pl.when((group == 0) & (sp > 0))
        def _():
            send_left.start()

        @pl.when(group == 0)
        def _():
            pass_on(near_z)

        @pl.when(group == 1)
        def _():
            pass_on(far_z)

        return carry

    lax.fori_loop(0, 2, project_group, 0)

    wo_sends[3].wait_recv()
    wo_sends[5].start()
    wo_sends[1].wait_recv()
    wo_sends[2].wait_recv()
    wo_sends[6].start()
    wo_sends[7].start()

    @pl.when(sp > 0)
    def _():
        send_right.wait_recv()

    @pl.when(sp < nsp - 1)
    def _():
        send_left.wait_recv()

    for sample in range(samples):
        store_values(kv_v[sample, :WINDOW].astype(f32).T, sample, ctx)
        store_values(kv_v[sample, WINDOW + tokens :].astype(f32).T, sample, ctx + WINDOW + tokens)
        vt_v[sample, :16, :] = jnp.ones((16, ctx + tokens + 2 * WINDOW), bf16)
    drain(ckv_v.at[:, pl.ds(0, nz * (nx - 1))], stage_sem.at[7])
    for sample in range(samples):
        store_values(ckv_v[sample].reshape(ctx, LANES).astype(f32).T, sample, 0)

    def att_copy(step_k, sample, dest):
        return remote(
            att_v.at[sample, pl.ds(pl.multiple_of(dest * chunk, chunk), chunk), :], by_v.at[tp, sample],
            att_send.at[step_k, sample], att_recv.at[step_k, sample], place(tp_to=dest),
        )

    limits_v[0:1, :] = jnp.concatenate([jnp.full((1, WINDOW), lift_ref[h] * LOG2E, f32) for h in range(4)], axis=1)
    limits_v[1:2, :] = jnp.concatenate([jnp.full((1, WINDOW), sink_ref[h] * LOG2E, f32) for h in range(4)], axis=1)
    subs = chunk // WINDOW
    deep_keys = min(256, ctx)
    pieces = [("far", c * deep_keys, c * deep_keys, deep_keys) for c in range(ctx // deep_keys)]
    pieces += [("near", c * WINDOW, ctx + c * WINDOW, WINDOW) for c in range(3)]
    buffers = ((s0_v, t0_v), (s1_v, t1_v))

    def rows_of(step, sub):
        k, sample = step // samples, step % samples
        dest = lax.rem(tp + 1 + k, nt)
        return sample, pl.multiple_of(dest * chunk + sub * WINDOW, WINDOW)

    def scores(step, buffer, sub):
        sample, row = rows_of(step, sub)
        left_off = jnp.where((sp == 0) & (row == 0), NEGATIVE, 0.0)
        right_off = jnp.where((sp == nsp - 1) & (row == tokens - WINDOW), NEGATIVE, 0.0)
        score_ref, top_ref = buffer
        return Scores((kv_v, ckv_v, q_v, limits_v), sample, row, left_off, right_off, score_ref.at[sub], top_ref.at[sub])

    def weights(step, buffer, sub):
        sample, row = rows_of(step, sub)
        score_ref, top_ref = buffer
        return Weights(vt_v, limits_v, att_v, ctx, sample, row, score_ref.at[sub], top_ref.at[sub])

    def both(now, later):
        for piece in pieces:
            for sub in range(subs):
                if now:
                    now[sub].piece(*piece)
                if later:
                    later[sub].piece(*piece)
        for sub in range(subs):
            if later:
                later[sub].done()
            if now:
                now[sub].done()

    both(None, [scores(0, buffers[0], sub) for sub in range(subs)])
    turns = nt * samples

    def chunk_step(step, carry):
        for parity in range(2):

            @pl.when(step % 2 == parity)
            def _():
                both(
                    [weights(step, buffers[parity], sub) for sub in range(subs)],
                    [scores(step + 1, buffers[1 - parity], sub) for sub in range(subs)],
                )

        k, sample = step // samples, step % samples

        @pl.when(k < nt - 1)
        def _():
            att_copy(k, sample, lax.rem(tp + 1 + k, nt)).start()

        @pl.when(step == 3)
        def _():
            wo_sends[4].wait_recv()
            wo_sends[5].wait_recv()
            wo_sends[8].start()

        return carry

    lax.fori_loop(0, turns - 1, chunk_step, 0)
    both([weights(turns - 1, buffers[(turns - 1) % 2], sub) for sub in range(subs)], None)
    by_v[tp] = att_v[:, pl.ds(pl.multiple_of(tp * chunk, chunk), chunk), :]

    for k in (6, 7, 8):
        wo_sends[k].wait_recv()
    for k in range(nt - 1):
        for sample in range(samples):
            att_copy(k, sample, lax.rem(tp + 1 + k, nt)).wait_recv()

    wide = min(1024, width)
    for sample in range(samples):

        def project_out(step, carry):
            cols = pl.ds(pl.multiple_of(step * wide, wide), wide)
            total = jnp.zeros((chunk, wide), f32)
            for t in range(nt):
                total = total + jnp.dot(
                    by_v[t, sample], wo_v[t * own_rows : (t + 1) * own_rows, cols], preferred_element_type=f32
                )
            out_v[sample, :, cols] = (total * modr_v[6 + sample : 7 + sample, cols]).astype(bf16)
            return carry

        lax.fori_loop(0, width // wide, project_out, 0)

    drain(rx_v, stage_sem.at[0])
    drain(rz_v, stage_sem.at[2])
    drain(mod_v.at[pl.ds(0, nt * nx - 1)], stage_sem.at[4])
    drain(ckv_v.at[:, pl.ds(0, nz * (nx - 1))], stage_sem.at[6])
    for offset in range(1, nz):
        ctx_along_z(offset).wait_send()
    for copy in wo_sends:
        copy.wait_send()

    @pl.when(sp < nsp - 1)
    def _():
        send_right.wait_send()

    @pl.when(sp > 0)
    def _():
        send_left.wait_send()

    for k in range(nt - 1):
        for sample in range(samples):
            att_copy(k, sample, lax.rem(tp + 1 + k, nt)).wait_send()


def shards(
    sizes, latent, context, condition, ctx_cond, norm_gain, w_shift, w_scale, w_gate, w_query, w_key, w_value, w_out,
    sink_logit, ctx_lift,
):
    nsp, nx, nt, nd = sizes
    nz = nsp // nx
    samples, tokens, width = latent.shape
    ctx_local = context.shape[1]
    ctx = ctx_local * nsp
    feats = condition.shape[1]
    cols = w_shift.shape[1]
    chunk = tokens // nt
    keys = ctx + tokens + 2 * WINDOW
    own_rows = w_out.shape[0]
    anywhere = pl.BlockSpec(memory_space=pltpu.HBM)
    vmem = pl.BlockSpec(memory_space=pltpu.VMEM)
    smem = pl.BlockSpec(memory_space=pltpu.SMEM)
    dma = pltpu.SemaphoreType.DMA
    return pl.pallas_call(
        functools.partial(layer, sizes),
        out_shape=pltpu.VMEM((samples, chunk, width), bf16),
        in_specs=[anywhere, anywhere, vmem, vmem, vmem] + [anywhere] * 7 + [smem, smem],
        out_specs=vmem,
        scratch_shapes=[
            pltpu.VMEM((samples, tokens, width), bf16),
            pltpu.VMEM((samples, ctx_local, width), bf16),
            pltpu.VMEM((3, feats, cols), bf16),
            pltpu.VMEM((width, 4 * HEAD), bf16),
            pltpu.VMEM((LANES, width), bf16),
            pltpu.VMEM((width, LANES), bf16),
            pltpu.VMEM((own_rows * nt, width), bf16),
            pltpu.VMEM((16, feats), f32),
            pltpu.VMEM((nx, 8, LANES), f32),
            pltpu.VMEM((nx - 1, 8, LANES), f32),
            pltpu.VMEM((8, LANES), f32),
            pltpu.VMEM((nz - 1, 8, LANES), f32),
            pltpu.VMEM((nt * nx, 8, LANES), f32),
            pltpu.VMEM((8, width), f32),
            pltpu.VMEM((samples, 8, width), f32),
            pltpu.VMEM((samples, 8, width), f32),
            pltpu.VMEM((samples, tokens, LANES), f32),
            pltpu.VMEM((tokens, LANES), f32),
            pltpu.VMEM((tokens, LANES), f32),
            pltpu.VMEM((samples, tokens, 4 * HEAD), bf16),
            pltpu.VMEM((samples, tokens + 2 * WINDOW, LANES), bf16),
            pltpu.VMEM((samples, nsp, ctx_local, LANES), bf16),
            pltpu.VMEM((samples, HEAD + 16, keys), bf16),
            pltpu.VMEM((8, 4 * WINDOW), f32),
            pltpu.VMEM((chunk // WINDOW, ctx + 3 * WINDOW, 4 * WINDOW), f32),
            pltpu.VMEM((chunk // WINDOW, ctx + 3 * WINDOW, 4 * WINDOW), f32),
            pltpu.VMEM((chunk // WINDOW, 8, 4 * WINDOW), f32),
            pltpu.VMEM((chunk // WINDOW, 8, 4 * WINDOW), f32),
            pltpu.VMEM((samples, tokens, 2 * LANES), bf16),
            pltpu.VMEM((nt, samples, chunk, 2 * LANES), bf16),
            dma((9,)),
            dma((8,)),
            dma((2, nz)),
            dma((2,)),
            dma((2,)),
            dma((9,)),
            dma((9,)),
            dma((nt - 1, samples)),
            dma((nt - 1, samples)),
        ],
        compiler_params=pltpu.CompilerParams(
            collective_id=0, has_side_effects=True, vmem_limit_bytes=61 * 1024 * 1024
        ),
        name="layer",
    )(
        latent, context, condition, ctx_cond.reshape(1, feats), norm_gain.reshape(1, width), w_shift, w_scale, w_gate,
        w_query, w_key.T, w_value.T, w_out, sink_logit, ctx_lift,
    )


def solution(mesh):
    nsp, nt, nd = mesh.shape["sp"], mesh.shape["tp"], mesh.shape["dp"]
    sizes = (nsp, 4 if nsp > 4 else 2, nt, nd)
    return jax.shard_map(
        functools.partial(shards, sizes),
        mesh=mesh,
        in_specs=(
            P("dp", "sp", None),
            P("dp", "sp", None),
            P("dp", "sp"),
            P("sp"),
            P(),
            P("sp", "tp"),
            P("sp", "tp"),
            P("sp", "tp"),
            P(None, "tp"),
            P(None, "tp"),
            P(None, "tp"),
            P("tp", None),
            P("tp"),
            P("tp"),
        ),
        out_specs=P("dp", ("sp", "tp"), None),
        check_vma=False,
    )
```

time: 72.1 us -> 54.9 us (0.76)
  Pallas kernels: 63.8 us -> 53 us
  local copies, waits for them, and re-layouts: 7.07 us -> 1.32 us
    pallas_call x1, Pallas kernels: 63.8 us -> 53 us  [shards(): pl.pallas_call(functools.partial(layer, sizes), out_shape=pltpu.VMEM((sam...]
    unnamed x3 -> x1, local copies, waits for them, and re-layouts: 7.07 us -> 1.32 us
where the time goes in v2:
time: 54.9 us; the launch traced here: 54.4 us
  Pallas kernels  53 us (97%)
  local copies, waits for them, and re-layouts  1.32 us (2%)
    pallas_call x1, Pallas kernels, shards(): pl.pallas_call(functools.partial(layer, sizes), out_shape=pltpu.VMEM((sam...  53 us
    unnamed x1, local copies, waits for them, and re-layouts  1.32 us

profile of v2, /device:TPU:32, one launch (start us, length us, event | category | flops | bytes accessed | tf_op | source)
XLA Modules:
  0.0 54.4 jit_solution(15407942876941069674)
XLA Ops:
  0.0 53.0 %layer.1 = bf16[2,256,2048]{2,1,0:T(8,128)(2,1)S(1)} custom-call(bf16[2,1024,2048]{2,1,0:T(8,128)(2,1)} %x_hbm.1, bf16[2,32,2048]{2,1,0:T(8,128)(2,1)} %context_hbm.1, bf16[2,64]{1,0:T(2,128)(2,1)} %condition.1, bf16[1,64]{1,0:T(2,128)(2,1)} %bitcast.7, f32[1,2048]{1,0:T(1,128)} %bitcast.6, bf16[64,512]{1,0:T(8,128)(2,1)} %wsh_hbm.1, ...), custom_call_target="tpu_custom_call" | custom-call | tf_op jit(solution)/shard_map/layer/pallas_call | solution.py:567
  53.0 1.3 %copy.16 = bf16[2,256,2048]{2,1,0:T(8,128)(2,1)} copy(bf16[2,256,2048]{2,1,0:T(8,128)(2,1)S(1)} %layer.1) | data formatting | bytes 4194304

commit v3 on v2

--- a/solution.py
+++ b/solution.py
@@ -320,17 +320,22 @@
         rows = ctx_rows_of(sp)
         return remote(rows, rows, ctx_sem.at[0, offset], ctx_sem.at[1, offset], place(sp_to=z_peer(offset)))
 
-    for offset in range(1, nz):
+    far_z = [offset for offset in range(1, nz) if 2 < offset < nz - 2]
+    near_z = [offset for offset in range(1, nz) if offset not in far_z]
+    for offset in near_z:
         ctx_along_z(offset).start()
     ctx_along_x(zi)
+    own_pairs = ctx_rows_of(sp)
+    for offset in far_z:
+        ctx_along_z(offset).start()
+        for dx in range(1, nx):
+            to = lax.rem(zi + offset, nz) * nx + lax.rem(xi + dx, nx)
+            remote(own_pairs, own_pairs, stage_sem.at[6], stage_sem.at[7], place(sp_to=to)).start()
 
     def pass_on(offsets):
         for offset in offsets:
             ctx_along_z(offset).wait_recv()
             ctx_along_x(lax.rem(zi + nz - offset, nz))
-
-    far_z = [offset for offset in range(1, nz) if 2 < offset < nz - 2]
-    near_z = [offset for offset in range(1, nz) if offset not in far_z]
 
     lane = lanes_of(block)
     low = lane < HEAD
@@ -397,10 +402,6 @@
         def _():
             pass_on(near_z)
 
-        @pl.when(group == 1)
-        def _():
-            pass_on(far_z)
-
         return carry
 
     lax.fori_loop(0, 2, project_group, 0)
@@ -424,11 +425,14 @@
         store_values(kv_v[sample, :WINDOW].astype(f32).T, sample, ctx)
         store_values(kv_v[sample, WINDOW + tokens :].astype(f32).T, sample, ctx + WINDOW + tokens)
         vt_v[sample, :16, :] = jnp.ones((16, ctx + tokens + 2 * WINDOW), bf16)
-    drain(ckv_v.at[:, pl.ds(0, nz * (nx - 1))], stage_sem.at[7])
-    for sample in range(samples):
-        store_values(ckv_v[sample].reshape(ctx, LANES).astype(f32).T, sample, 0)
-
-    def att_copy(step_k, sample, dest):
+    assert nt == 4
+
+    def destination(k):
+        late = k // 2
+        return lax.rem(tp + (1 - late) * (2 - k) + late * (9 - 3 * k), nt)
+
+    def att_copy(step_k, sample):
+        dest = destination(step_k)
         return remote(
             att_v.at[sample, pl.ds(pl.multiple_of(dest * chunk, chunk), chunk), :], by_v.at[tp, sample],
             att_send.at[step_k, sample], att_recv.at[step_k, sample], place(tp_to=dest),
@@ -444,7 +448,7 @@
 
     def rows_of(step, sub):
         k, sample = step // samples, step % samples
-        dest = lax.rem(tp + 1 + k, nt)
+        dest = destination(k)
         return sample, pl.multiple_of(dest * chunk + sub * WINDOW, WINDOW)
 
     def scores(step, buffer, sub):
@@ -459,20 +463,30 @@
         score_ref, top_ref = buffer
         return Weights(vt_v, limits_v, att_v, ctx, sample, row, score_ref.at[sub], top_ref.at[sub])
 
-    def both(now, later):
+    def both(now, later, only="all"):
         for piece in pieces:
             for sub in range(subs):
-                if now:
+                if now and only == "all":
                     now[sub].piece(*piece)
-                if later:
+                if later and only in ("all", piece[0]):
                     later[sub].piece(*piece)
-        for sub in range(subs):
+        for sub in range(subs if only in ("all", None) else 0):
             if later:
                 later[sub].done()
             if now:
                 now[sub].done()
 
-    both(None, [scores(0, buffers[0], sub) for sub in range(subs)])
+    start = [scores(0, buffers[0], sub) for sub in range(subs)]
+    both(None, start, "near")
+
+    for offset in far_z:
+        ctx_along_z(offset).wait_recv()
+    drain(ckv_v.at[:, pl.ds(0, nz * (nx - 1))], stage_sem.at[7])
+    for sample in range(samples):
+        store_values(ckv_v[sample].reshape(ctx, LANES).astype(f32).T, sample, 0)
+
+    both(None, start, "far")
+    both(None, start, None)
     turns = nt * samples
 
     def chunk_step(step, carry):
@@ -489,7 +503,7 @@
 
         @pl.when(k < nt - 1)
         def _():
-            att_copy(k, sample, lax.rem(tp + 1 + k, nt)).start()
+            att_copy(k, sample).start()
 
         @pl.when(step == 3)
         def _():
@@ -505,12 +519,10 @@
 
     for k in (6, 7, 8):
         wo_sends[k].wait_recv()
-    for k in range(nt - 1):
-        for sample in range(samples):
-            att_copy(k, sample, lax.rem(tp + 1 + k, nt)).wait_recv()
-
     wide = min(1024, width)
     for sample in range(samples):
+        for k in range(nt - 1):
+            att_copy(k, sample).wait_recv()
 
         def project_out(step, carry):
             cols = pl.ds(pl.multiple_of(step * wide, wide), wide)
@@ -543,7 +555,7 @@
 
     for k in range(nt - 1):
         for sample in range(samples):
-            att_copy(k, sample, lax.rem(tp + 1 + k, nt)).wait_send()
+            att_copy(k, sample).wait_send()
 
 
 def shards(

time: 54.9 us -> 51 us (0.929)
  Pallas kernels: 53 us -> 49 us
    pallas_call x1, Pallas kernels: 53 us -> 49 us  [shards(): pl.pallas_call(functools.partial(layer, sizes), out_shape=pltpu.VMEM((sam...]
where the time goes in v3:
time: 51 us; the launch traced here: 50.3 us
  Pallas kernels  49 us (96%)
  local copies, waits for them, and re-layouts  1.32 us (3%)
    pallas_call x1, Pallas kernels, shards(): pl.pallas_call(functools.partial(layer, sizes), out_shape=pltpu.VMEM((sam...  49 us
    unnamed x1, local copies, waits for them, and re-layouts  1.32 us

profile of v3, /device:TPU:32, one launch (start us, length us, event | category | flops | bytes accessed | tf_op | source)
XLA Modules:
  0.0 50.3 jit_solution(11027884134740549979)
XLA Ops:
  0.0 49.0 %layer.1 = bf16[2,256,2048]{2,1,0:T(8,128)(2,1)S(1)} custom-call(bf16[2,1024,2048]{2,1,0:T(8,128)(2,1)} %x_hbm.1, bf16[2,32,2048]{2,1,0:T(8,128)(2,1)} %context_hbm.1, bf16[2,64]{1,0:T(2,128)(2,1)} %condition.1, bf16[1,64]{1,0:T(2,128)(2,1)} %bitcast.7, f32[1,2048]{1,0:T(1,128)} %bitcast.6, bf16[64,512]{1,0:T(8,128)(2,1)} %wsh_hbm.1, ...), custom_call_target="tpu_custom_call" | custom-call | tf_op jit(solution)/shard_map/layer/pallas_call | solution.py:579
  49.0 1.3 %copy.16 = bf16[2,256,2048]{2,1,0:T(8,128)(2,1)} copy(bf16[2,256,2048]{2,1,0:T(8,128)(2,1)S(1)} %layer.1) | data formatting | bytes 4194304

commit v4 on v3

--- a/solution.py
+++ b/solution.py
@@ -89,10 +89,10 @@
 
 def layer(
     sizes,
-    x_hbm, context_hbm, condition, ctx_cond, gain, wsh_hbm, wsc_hbm, wga_hbm, wq_hbm, wk_hbm, wv_hbm, wo_hbm,
-    sink_ref, lift_ref,
+    x_hbm, context_hbm, condition_hbm, ctx_cond_hbm, gain_hbm, wsh_hbm, wsc_hbm, wga_hbm, wq_hbm, wk_hbm, wv_hbm, wo_hbm,
+    sink_hbm, lift_hbm,
     out_v,
-    x_v, context_v, wm_v, wq_v, wt_v, wkv_v, wo_v,
+    condition, ctx_cond, gain, sink_ref, lift_ref, x_v, context_v, wm_v, wq_v, wt_v, wkv_v, wo_v,
     active_v, part_v, rx_v, zsrc_v, rz_v, mod_v, modr_v, mul_v, add_v,
     inv_v, cos_v, sin_v, q_v, kv_v, ckv_v, vt_v, limits_v, s0_v, s1_v, t0_v, t1_v, att_v, by_v,
     local_sem, stage_sem, ctx_sem, halo_send, halo_recv, wo_send, wo_recv, att_send, att_recv,
@@ -142,7 +142,14 @@
         pltpu.make_async_copy(wv_hbm, wt_v.at[pl.ds(HEAD, HEAD), :], local_sem.at[7]),
         pltpu.make_async_copy(wq_hbm, wq_v, local_sem.at[8]),
     ]
-    for load in loads:
+    small = [
+        pltpu.make_async_copy(condition_hbm, condition, local_sem.at[9]),
+        pltpu.make_async_copy(ctx_cond_hbm, ctx_cond, local_sem.at[10]),
+        pltpu.make_async_copy(gain_hbm, gain, local_sem.at[11]),
+        pltpu.make_async_copy(sink_hbm, sink_ref, local_sem.at[12]),
+        pltpu.make_async_copy(lift_hbm, lift_ref, local_sem.at[13]),
+    ]
+    for load in small[:2] + loads + small[2:]:
         load.start()
 
     barrier = pltpu.get_barrier_semaphore()
@@ -160,6 +167,8 @@
         greet(place(dp_to=lax.rem(dp + offset, nd)))
 
     active_v[...] = jnp.zeros_like(active_v)
+    for load in small[:2]:
+        load.wait()
     active_v[0:2, :] = condition[...].astype(f32)
     active_v[2:3, :] = ctx_cond[...].astype(f32)
     raw = active_v[...]
@@ -299,6 +308,7 @@
     drain(mod_v.at[pl.ds(0, nt * nx - 1)], stage_sem.at[5])
     for k in range(nt * nx):
         modr_v[:, k * LANES : (k + 1) * LANES] = mod_v[k]
+    small[2].wait()
     scaled = gain[...] * (1.0 + modr_v[3:6, :])
     for r in range(samples):
         mul_v[r, 0:1, :] = scaled[r : r + 1]
@@ -438,8 +448,12 @@
             att_send.at[step_k, sample], att_recv.at[step_k, sample], place(tp_to=dest),
         )
 
-    limits_v[0:1, :] = jnp.concatenate([jnp.full((1, WINDOW), lift_ref[h] * LOG2E, f32) for h in range(4)], axis=1)
-    limits_v[1:2, :] = jnp.concatenate([jnp.full((1, WINDOW), sink_ref[h] * LOG2E, f32) for h in range(4)], axis=1)
+    for load, ref, line in ((small[4], lift_ref, 0), (small[3], sink_ref, 1)):
+        load.wait()
+        for h in range(4):
+            limits_v[line : line + 1, h * WINDOW : (h + 1) * WINDOW] = jnp.broadcast_to(
+                ref[0:1, h : h + 1] * LOG2E, (1, WINDOW)
+            )
     subs = chunk // WINDOW
     deep_keys = min(256, ctx)
     pieces = [("far", c * deep_keys, c * deep_keys, deep_keys) for c in range(ctx // deep_keys)]
@@ -519,7 +533,7 @@
 
     for k in (6, 7, 8):
         wo_sends[k].wait_recv()
-    wide = min(1024, width)
+    wide = width
     for sample in range(samples):
         for k in range(nt - 1):
             att_copy(k, sample).wait_recv()
@@ -574,14 +588,18 @@
     own_rows = w_out.shape[0]
     anywhere = pl.BlockSpec(memory_space=pltpu.HBM)
     vmem = pl.BlockSpec(memory_space=pltpu.VMEM)
-    smem = pl.BlockSpec(memory_space=pltpu.SMEM)
     dma = pltpu.SemaphoreType.DMA
     return pl.pallas_call(
         functools.partial(layer, sizes),
         out_shape=pltpu.VMEM((samples, chunk, width), bf16),
-        in_specs=[anywhere, anywhere, vmem, vmem, vmem] + [anywhere] * 7 + [smem, smem],
+        in_specs=[anywhere] * 14,
         out_specs=vmem,
         scratch_shapes=[
+            pltpu.VMEM((samples, feats), bf16),
+            pltpu.VMEM((1, feats), bf16),
+            pltpu.VMEM((1, width), f32),
+            pltpu.VMEM((1, 4), f32),
+            pltpu.VMEM((1, 4), f32),
             pltpu.VMEM((samples, tokens, width), bf16),
             pltpu.VMEM((samples, ctx_local, width), bf16),
             pltpu.VMEM((3, feats, cols), bf16),
@@ -612,7 +630,7 @@
             pltpu.VMEM((chunk // WINDOW, 8, 4 * WINDOW), f32),
             pltpu.VMEM((samples, tokens, 2 * LANES), bf16),
             pltpu.VMEM((nt, samples, chunk, 2 * LANES), bf16),
-            dma((9,)),
+            dma((14,)),
             dma((8,)),
             dma((2, nz)),
             dma((2,)),
@@ -628,7 +646,7 @@
         name="layer",
     )(
         latent, context, condition, ctx_cond.reshape(1, feats), norm_gain.reshape(1, width), w_shift, w_scale, w_gate,
-        w_query, w_key.T, w_value.T, w_out, sink_logit, ctx_lift,
+        w_query, w_key.T, w_value.T, w_out, sink_logit.reshape(1, 4), ctx_lift.reshape(1, 4),
     )
 
 

time: 51 us -> 49.8 us (0.976)
  Pallas kernels: 49 us -> 47.7 us
    pallas_call x1, Pallas kernels: 49 us -> 47.7 us  [shards(): pl.pallas_call(functools.partial(layer, sizes), out_shape=pltpu.VMEM((sam...]
where the time goes in v4:
time: 49.8 us; the launch traced here: 49.1 us
  Pallas kernels  47.7 us (96%)
  local copies, waits for them, and re-layouts  1.32 us (3%)
    pallas_call x1, Pallas kernels, shards(): pl.pallas_call(functools.partial(layer, sizes), out_shape=pltpu.VMEM((sam...  47.7 us
    unnamed x1, local copies, waits for them, and re-layouts  1.32 us

profile of v4, /device:TPU:32, one launch (start us, length us, event | category | flops | bytes accessed | tf_op | source)
XLA Modules:
  0.0 49.1 jit_solution(13688128011519010674)
XLA Ops:
  0.0 47.7 %layer.1 = bf16[2,256,2048]{2,1,0:T(8,128)(2,1)S(1)} custom-call(bf16[2,1024,2048]{2,1,0:T(8,128)(2,1)} %x_hbm.1, bf16[2,32,2048]{2,1,0:T(8,128)(2,1)} %context_hbm.1, bf16[2,64]{1,0:T(2,128)(2,1)} %condition_hbm.1, bf16[1,64]{1,0:T(2,128)(2,1)} %bitcast.9, f32[1,2048]{1,0:T(1,128)} %bitcast.8, bf16[64,512]{1,0:T(8,128)(2,1)} %wsh_hbm.1, ...), custom_call_target="tpu_custom_call" | custom-call | tf_op jit(solution)/shard_map/layer/pallas_call | solution.py:592
  47.8 1.3 %copy.16 = bf16[2,256,2048]{2,1,0:T(8,128)(2,1)} copy(bf16[2,256,2048]{2,1,0:T(8,128)(2,1)S(1)} %layer.1) | data formatting | bytes 4194304

commit v5 on v4

--- a/solution.py
+++ b/solution.py
@@ -34,51 +34,51 @@
 
 
 class Scores:
-    def __init__(self, refs, sample, row, left_off, right_off, score_ref, top_ref):
-        self.kv, self.ckv, q_ref, self.limits = refs
-        self.sample, self.row, self.offsets = sample, row, {0: left_off, 2 * WINDOW: right_off}
-        self.score_ref, self.top_ref = score_ref, top_ref
+    def __init__(self, kv, ckv, q_ref, sample, row):
+        self.kv, self.ckv, self.sample, self.row = kv, ckv, sample, row
         turned = q_ref[sample, pl.ds(row, WINDOW), :].astype(f32).T.astype(bf16)
         self.q = jnp.concatenate([turned[h * HEAD : (h + 1) * HEAD] for h in range(4)], axis=1)
-        self.tops = {}
-
-    def piece(self, kind, at, put, rows):
-        ctx_local = self.ckv.shape[2]
-        if kind == "far":
-            keys = self.ckv[self.sample, at // ctx_local : (at + rows) // ctx_local].reshape(rows, LANES)
-        else:
-            keys = self.kv[self.sample, pl.ds(pl.multiple_of(self.row + at, WINDOW), rows), :]
+        self.top = None
+
+    def put(self, score, score_ref, at):
+        rows = score.shape[0]
+        score_ref[at : at + rows, :] = score
+        top = jnp.max(score.reshape(rows // 8, 8, score.shape[1]), axis=0)
+        self.top = top if self.top is None else jnp.maximum(self.top, top)
+
+    def far(self, at, rows, score_ref):
+        local = self.ckv.shape[2]
+        keys = self.ckv[self.sample, at // local : (at + rows) // local].reshape(rows, LANES)
+        self.put(jnp.dot(keys[:, :HEAD], self.q, preferred_element_type=f32), score_ref, at)
+
+    def near(self, at, score_ref, offset):
+        keys = self.kv[self.sample, pl.ds(pl.multiple_of(self.row + at, WINDOW), WINDOW), :]
         score = jnp.dot(keys[:, :HEAD], self.q, preferred_element_type=f32)
-        if kind == "near" and at != WINDOW:
+        if at != WINDOW:
             key = lax.broadcasted_iota(jnp.int32, score.shape, 0)
             query = lax.broadcasted_iota(jnp.int32, score.shape, 1) % WINDOW
             inside = key >= query if at == 0 else key <= query
-            score = jnp.where(inside, score, NEGATIVE) + self.offsets[at]
-        self.score_ref[put : put + rows, :] = score
-        top = jnp.max(score.reshape(rows // 8, 8, score.shape[1]), axis=0)
-        self.tops[kind] = jnp.maximum(self.tops[kind], top) if kind in self.tops else top
-
-    def done(self):
-        far = jnp.max(self.tops["far"], axis=0, keepdims=True) + self.limits[0:1, :]
-        near = jnp.max(self.tops["near"], axis=0, keepdims=True)
-        self.top_ref[0:1, :] = jnp.maximum(jnp.maximum(far, near), self.limits[1:2, :])
+            score = jnp.where(inside, score, NEGATIVE) + offset
+        self.put(score, score_ref, at)
 
 
 class Weights:
-    def __init__(self, vt, limits, att, ctx, sample, row, score_ref, top_ref):
+    def __init__(self, vt, limits, att, ctx, sample, row, score_ref, near_ref, top_ref):
         self.vt, self.att, self.ctx, self.sample, self.row, self.score_ref = vt, att, ctx, sample, row, score_ref
+        self.near_ref = near_ref
         self.top = top_ref[0:1, :]
         self.lowered = self.top - limits[0:1, :]
         self.sink = jnp.exp2(limits[1:2, :] - self.top)
         self.total = jnp.zeros((vt.shape[1], 4 * WINDOW), f32)
 
-    def piece(self, kind, at, put, rows):
-        top = self.lowered if kind == "far" else self.top
-        weight = jnp.exp2(self.score_ref[put : put + rows, :] - top).astype(bf16)
+    def piece(self, kind, at, rows):
         if kind == "far":
+            score, top = self.score_ref[at : at + rows, :], self.lowered
             values = self.vt[self.sample, :, at : at + rows]
         else:
+            score, top = self.near_ref[at : at + rows, :], self.top
             values = self.vt[self.sample, :, pl.ds(pl.multiple_of(self.ctx + self.row + at, WINDOW), rows)]
+        weight = jnp.exp2(score - top).astype(bf16)
         self.total = self.total + jnp.dot(values, weight, preferred_element_type=f32)
 
     def done(self):
@@ -87,14 +87,38 @@
         self.att[self.sample, pl.ds(self.row, WINDOW), :] = stacked.T.astype(bf16)
 
 
+def gated(by_v, wo_v, modr_v, sample, cols):
+    owners = by_v.shape[0]
+    rows = wo_v.shape[0] // owners
+    total = jnp.zeros((by_v.shape[2], modr_v[0:1, cols].shape[1]), f32)
+    for t in range(owners):
+        total = total + jnp.dot(
+            by_v[t, sample], wo_v[t * rows : (t + 1) * rows, cols], preferred_element_type=f32
+        )
+    return (total * modr_v[6 + sample : 7 + sample, cols]).astype(bf16)
+
+
+def closing(first_v, by_v, wo_v, modr_v, out_hbm, last_v, sem):
+    copies = [pltpu.make_async_copy(first_v, out_hbm.at[0], sem.at[0])]
+    copies[0].start()
+    wide = last_v.shape[1] // 4
+    for n in range(4):
+        cols = slice(n * wide, (n + 1) * wide)
+        last_v[:, cols] = gated(by_v, wo_v, modr_v, 1, cols)
+        copies.append(pltpu.make_async_copy(last_v.at[:, cols], out_hbm.at[1, :, cols], sem.at[1 + n]))
+        copies[-1].start()
+    for copy in copies:
+        copy.wait()
+
+
 def layer(
     sizes,
     x_hbm, context_hbm, condition_hbm, ctx_cond_hbm, gain_hbm, wsh_hbm, wsc_hbm, wga_hbm, wq_hbm, wk_hbm, wv_hbm, wo_hbm,
     sink_hbm, lift_hbm,
-    out_v,
-    condition, ctx_cond, gain, sink_ref, lift_ref, x_v, context_v, wm_v, wq_v, wt_v, wkv_v, wo_v,
-    active_v, part_v, rx_v, zsrc_v, rz_v, mod_v, modr_v, mul_v, add_v,
-    inv_v, cos_v, sin_v, q_v, kv_v, ckv_v, vt_v, limits_v, s0_v, s1_v, t0_v, t1_v, att_v, by_v,
+    out_v, by_v, wo_v, modr_v,
+    condition, ctx_cond, gain, sink_ref, lift_ref, x_v, context_v, wm_v, wq_v, wt_v, wkv_v,
+    active_v, part_v, rx_v, zsrc_v, rz_v, mod_v, mul_v, add_v,
+    inv_v, cos_v, sin_v, q_v, kv_v, ckv_v, vt_v, limits_v, near_v, near_top_v, s0_v, s1_v, t0_v, t1_v, att_v,
     local_sem, stage_sem, ctx_sem, halo_send, halo_recv, wo_send, wo_recv, att_send, att_recv,
 ):
     nsp, nx, nt, nd = sizes
@@ -149,7 +173,7 @@
         pltpu.make_async_copy(sink_hbm, sink_ref, local_sem.at[12]),
         pltpu.make_async_copy(lift_hbm, lift_ref, local_sem.at[13]),
     ]
-    for load in small[:2] + loads + small[2:]:
+    for load in small[:2] + loads[:3] + loads[6:8] + loads[3:5] + loads[8:] + small[2:] + loads[5:6]:
         load.start()
 
     barrier = pltpu.get_barrier_semaphore()
@@ -228,11 +252,6 @@
         mean = jnp.sum(total, axis=1, keepdims=True) / width
         inv_v[sample, pl.ds(start, block), :] = jnp.broadcast_to(lax.rsqrt(mean + EPSILON), (block, LANES))
 
-    loads[6].wait()
-    loads[7].wait()
-    wkv_v[...] = wt_v[...].T
-    loads[5].wait()
-
     def stats_loop(first, last):
         def run(step, carry):
             statistics(step)
@@ -241,18 +260,9 @@
         lax.fori_loop(first, last, run, 0)
 
     all_blocks = samples * blocks
-    stats_loop(0, all_blocks // 2)
-
-    drain(rx_v, stage_sem.at[1])
-    quarter_sum = part_v[xi]
-    for k in range(nx - 1):
-        quarter_sum = quarter_sum + rx_v[k]
-    zsrc_v[...] = quarter_sum
-
-    for offset in range(1, nz):
-        remote(zsrc_v, rz_v.at[offset - 1], stage_sem.at[2], stage_sem.at[3], place(sp_to=z_peer(offset))).start()
-
-    stats_loop(all_blocks // 2, all_blocks)
+    loads[6].wait()
+    loads[7].wait()
+    wkv_v[...] = wt_v[...].T
     lane1 = lanes_of(8)
     frequency = jnp.exp((lane1[0:1] % 16).astype(f32) * (-math.log(ROPE_BASE) / 16.0))
     grid_rows = tokens // GRID_COLS
@@ -270,6 +280,17 @@
         sine = jnp.where(by_row, row_sin[t : t + 1, :], col_sin)
         sin_v[rows, :] = jnp.where(minus, -sine, sine)
 
+    drain(rx_v, stage_sem.at[1])
+    quarter_sum = part_v[xi]
+    for k in range(nx - 1):
+        quarter_sum = quarter_sum + rx_v[k]
+    zsrc_v[...] = quarter_sum
+
+    for offset in range(1, nz):
+        remote(zsrc_v, rz_v.at[offset - 1], stage_sem.at[2], stage_sem.at[3], place(sp_to=z_peer(offset))).start()
+
+    loads[5].wait()
+    stats_loop(0, all_blocks // 2)
     drain(rz_v, stage_sem.at[3])
     total = zsrc_v[...]
     for k in range(nz - 1):
@@ -285,10 +306,10 @@
                     place(sp_to=x_peer(dx), tp_to=lax.rem(tp + dy, nt)),
                 ).start()
 
+    wo_sends[2].start()
+    wo_sends[3].start()
     wo_sends[0].wait_recv()
     wo_sends[4].start()
-    wo_sends[2].start()
-    wo_sends[3].start()
 
     @pl.when(sp == 0)
     def _():
@@ -305,6 +326,7 @@
     ctx_inv = lax.rsqrt(jnp.mean(ctx_wide * ctx_wide, axis=1, keepdims=True) + EPSILON)
     ctx_unit = ctx_wide * ctx_inv
 
+    stats_loop(all_blocks // 2, all_blocks)
     drain(mod_v.at[pl.ds(0, nt * nx - 1)], stage_sem.at[5])
     for k in range(nt * nx):
         modr_v[:, k * LANES : (k + 1) * LANES] = mod_v[k]
@@ -330,9 +352,10 @@
         rows = ctx_rows_of(sp)
         return remote(rows, rows, ctx_sem.at[0, offset], ctx_sem.at[1, offset], place(sp_to=z_peer(offset)))
 
-    far_z = [offset for offset in range(1, nz) if 2 < offset < nz - 2]
-    near_z = [offset for offset in range(1, nz) if offset not in far_z]
-    for offset in near_z:
+    far_z = [nz // 2]
+    near_z = [offset for offset in range(1, nz) if min(offset, nz - offset) < min(3, nz // 2)]
+    mid_z = [offset for offset in range(1, nz) if offset not in near_z + far_z]
+    for offset in near_z + mid_z:
         ctx_along_z(offset).start()
     ctx_along_x(zi)
     own_pairs = ctx_rows_of(sp)
@@ -396,45 +419,31 @@
         halo_recv.at[1], place(sp_to=lax.rem(sp + nsp - 1, nsp)),
     )
 
-    def project_group(group, carry):
-        for member in range(4):
-            project(4 * group + member)
-
-        @pl.when((group == 0) & (sp < nsp - 1))
-        def _():
-            send_right.start()
-
-        @pl.when((group == 0) & (sp > 0))
-        def _():
-            send_left.start()
-
-        @pl.when(group == 0)
-        def _():
-            pass_on(near_z)
-
-        return carry
-
-    lax.fori_loop(0, 2, project_group, 0)
-
+    def project_some(first, count):
+        def run(group, carry):
+            for member in range(count):
+                project(first + count * group + member)
+            return carry
+
+        lax.fori_loop(0, 1, run, 0)
+
+    project_some(0, 4)
+
+    @pl.when(sp < nsp - 1)
+    def _():
+        send_right.start()
+
+    @pl.when(sp > 0)
+    def _():
+        send_left.start()
+
+    project_some(4, 2)
+    pass_on(near_z)
     wo_sends[3].wait_recv()
     wo_sends[5].start()
-    wo_sends[1].wait_recv()
-    wo_sends[2].wait_recv()
-    wo_sends[6].start()
-    wo_sends[7].start()
-
-    @pl.when(sp > 0)
-    def _():
-        send_right.wait_recv()
-
-    @pl.when(sp < nsp - 1)
-    def _():
-        send_left.wait_recv()
-
-    for sample in range(samples):
-        store_values(kv_v[sample, :WINDOW].astype(f32).T, sample, ctx)
-        store_values(kv_v[sample, WINDOW + tokens :].astype(f32).T, sample, ctx + WINDOW + tokens)
-        vt_v[sample, :16, :] = jnp.ones((16, ctx + tokens + 2 * WINDOW), bf16)
+    project_some(6, 2)
+    pass_on(mid_z)
+
     assert nt == 4
 
     def destination(k):
@@ -456,8 +465,8 @@
             )
     subs = chunk // WINDOW
     deep_keys = min(256, ctx)
-    pieces = [("far", c * deep_keys, c * deep_keys, deep_keys) for c in range(ctx // deep_keys)]
-    pieces += [("near", c * WINDOW, ctx + c * WINDOW, WINDOW) for c in range(3)]
+    pieces = [("far", c * deep_keys, deep_keys) for c in range(ctx // deep_keys)]
+    pieces += [("near", c * WINDOW, WINDOW) for c in range(3)]
     buffers = ((s0_v, t0_v), (s1_v, t1_v))
 
     def rows_of(step, sub):
@@ -465,33 +474,44 @@
         dest = destination(k)
         return sample, pl.multiple_of(dest * chunk + sub * WINDOW, WINDOW)
 
-    def scores(step, buffer, sub):
-        sample, row = rows_of(step, sub)
-        left_off = jnp.where((sp == 0) & (row == 0), NEGATIVE, 0.0)
-        right_off = jnp.where((sp == nsp - 1) & (row == tokens - WINDOW), NEGATIVE, 0.0)
-        score_ref, top_ref = buffer
-        return Scores((kv_v, ckv_v, q_v, limits_v), sample, row, left_off, right_off, score_ref.at[sub], top_ref.at[sub])
-
-    def weights(step, buffer, sub):
-        sample, row = rows_of(step, sub)
-        score_ref, top_ref = buffer
-        return Weights(vt_v, limits_v, att_v, ctx, sample, row, score_ref.at[sub], top_ref.at[sub])
-
-    def both(now, later, only="all"):
-        for piece in pieces:
-            for sub in range(subs):
-                if now and only == "all":
-                    now[sub].piece(*piece)
-                if later and only in ("all", piece[0]):
-                    later[sub].piece(*piece)
-        for sub in range(subs if only in ("all", None) else 0):
-            if later:
-                later[sub].done()
-            if now:
-                now[sub].done()
-
-    start = [scores(0, buffers[0], sub) for sub in range(subs)]
-    both(None, start, "near")
+    def near_scores(sample, dest):
+        place_of = dest * samples + sample
+        for sub in range(subs):
+            row = pl.multiple_of(dest * chunk + sub * WINDOW, WINDOW)
+            left_off = jnp.where((sp == 0) & (row == 0), NEGATIVE, 0.0)
+            right_off = jnp.where((sp == nsp - 1) & (row == tokens - WINDOW), NEGATIVE, 0.0)
+            score = Scores(kv_v, ckv_v, q_v, sample, row)
+            for at, offset in ((0, left_off), (WINDOW, 0.0), (2 * WINDOW, right_off)):
+                score.near(at, near_v.at[place_of, sub], offset)
+            near_top_v[place_of, sub] = score.top
+
+    def near_of(step):
+        k, sample = step // samples, step % samples
+        return destination(k) * samples + sample
+
+    def near_pair(first, apart):
+        def run(turn, carry):
+            for sample in range(samples):
+                near_scores(sample, first + apart * turn)
+            return carry
+
+        lax.fori_loop(0, 2, run, 0)
+
+    near_pair(1, 1)
+
+    @pl.when(sp > 0)
+    def _():
+        send_right.wait_recv()
+
+    @pl.when(sp < nsp - 1)
+    def _():
+        send_left.wait_recv()
+
+    for sample in range(samples):
+        store_values(kv_v[sample, :WINDOW].astype(f32).T, sample, ctx)
+        store_values(kv_v[sample, WINDOW + tokens :].astype(f32).T, sample, ctx + WINDOW + tokens)
+        vt_v[sample, :16, :] = jnp.ones((16, ctx + tokens + 2 * WINDOW), bf16)
+    near_pair(0, nt - 1)
 
     for offset in far_z:
         ctx_along_z(offset).wait_recv()
@@ -499,8 +519,34 @@
     for sample in range(samples):
         store_values(ckv_v[sample].reshape(ctx, LANES).astype(f32).T, sample, 0)
 
-    both(None, start, "far")
-    both(None, start, None)
+
+    def scores(step, sub):
+        sample, row = rows_of(step, sub)
+        return Scores(kv_v, ckv_v, q_v, sample, row)
+
+    def weights(step, buffer, sub):
+        sample, row = rows_of(step, sub)
+        score_ref, top_ref = buffer
+        return Weights(
+            vt_v, limits_v, att_v, ctx, sample, row, score_ref.at[sub], near_v.at[near_of(step), sub], top_ref.at[sub]
+        )
+
+    def both(now, later, step, buffer):
+        for kind, at, rows in pieces:
+            for sub in range(subs):
+                if now:
+                    now[sub].piece(kind, at, rows)
+                if later and kind == "far":
+                    later[sub].far(at, rows, buffer[0].at[sub])
+        for sub in range(subs):
+            if later:
+                far = jnp.max(later[sub].top, axis=0, keepdims=True) + limits_v[0:1, :]
+                near = jnp.max(near_top_v[near_of(step), sub], axis=0, keepdims=True)
+                buffer[1][sub, 0:1, :] = jnp.maximum(jnp.maximum(far, near), limits_v[1:2, :])
+            if now:
+                now[sub].done()
+
+    both(None, [scores(0, sub) for sub in range(subs)], 0, buffers[0])
     turns = nt * samples
 
     def chunk_step(step, carry):
@@ -510,7 +556,9 @@
             def _():
                 both(
                     [weights(step, buffers[parity], sub) for sub in range(subs)],
-                    [scores(step + 1, buffers[1 - parity], sub) for sub in range(subs)],
+                    [scores(step + 1, sub) for sub in range(subs)],
+                    step + 1,
+                    buffers[1 - parity],
                 )
 
         k, sample = step // samples, step % samples
@@ -518,6 +566,13 @@
         @pl.when(k < nt - 1)
         def _():
             att_copy(k, sample).start()
+
+        @pl.when(step == 1)
+        def _():
+            wo_sends[1].wait_recv()
+            wo_sends[2].wait_recv()
+            wo_sends[6].start()
+            wo_sends[7].start()
 
         @pl.when(step == 3)
         def _():
@@ -528,27 +583,17 @@
         return carry
 
     lax.fori_loop(0, turns - 1, chunk_step, 0)
-    both([weights(turns - 1, buffers[(turns - 1) % 2], sub) for sub in range(subs)], None)
+    both([weights(turns - 1, buffers[(turns - 1) % 2], sub) for sub in range(subs)], None, None, None)
     by_v[tp] = att_v[:, pl.ds(pl.multiple_of(tp * chunk, chunk), chunk), :]
 
     for k in (6, 7, 8):
         wo_sends[k].wait_recv()
-    wide = width
-    for sample in range(samples):
+    for k in range(nt - 1):
+        att_copy(k, 0).wait_recv()
+    out_v[...] = gated(by_v, wo_v, modr_v, 0, slice(0, width))
+    for sample in range(1, samples):
         for k in range(nt - 1):
             att_copy(k, sample).wait_recv()
-
-        def project_out(step, carry):
-            cols = pl.ds(pl.multiple_of(step * wide, wide), wide)
-            total = jnp.zeros((chunk, wide), f32)
-            for t in range(nt):
-                total = total + jnp.dot(
-                    by_v[t, sample], wo_v[t * own_rows : (t + 1) * own_rows, cols], preferred_element_type=f32
-                )
-            out_v[sample, :, cols] = (total * modr_v[6 + sample : 7 + sample, cols]).astype(bf16)
-            return carry
-
-        lax.fori_loop(0, width // wide, project_out, 0)
 
     drain(rx_v, stage_sem.at[0])
     drain(rz_v, stage_sem.at[2])
@@ -589,11 +634,16 @@
     anywhere = pl.BlockSpec(memory_space=pltpu.HBM)
     vmem = pl.BlockSpec(memory_space=pltpu.VMEM)
     dma = pltpu.SemaphoreType.DMA
-    return pl.pallas_call(
+    kept = pl.pallas_call(
         functools.partial(layer, sizes),
-        out_shape=pltpu.VMEM((samples, chunk, width), bf16),
+        out_shape=(
+            pltpu.VMEM((chunk, width), bf16),
+            pltpu.VMEM((nt, samples, chunk, 2 * LANES), bf16),
+            pltpu.VMEM((own_rows * nt, width), bf16),
+            pltpu.VMEM((8, width), f32),
+        ),
         in_specs=[anywhere] * 14,
-        out_specs=vmem,
+        out_specs=(vmem,) * 4,
         scratch_shapes=[
             pltpu.VMEM((samples, feats), bf16),
             pltpu.VMEM((1, feats), bf16),
@@ -606,14 +656,12 @@
             pltpu.VMEM((width, 4 * HEAD), bf16),
             pltpu.VMEM((LANES, width), bf16),
             pltpu.VMEM((width, LANES), bf16),
-            pltpu.VMEM((own_rows * nt, width), bf16),
             pltpu.VMEM((16, feats), f32),
             pltpu.VMEM((nx, 8, LANES), f32),
             pltpu.VMEM((nx - 1, 8, LANES), f32),
             pltpu.VMEM((8, LANES), f32),
             pltpu.VMEM((nz - 1, 8, LANES), f32),
             pltpu.VMEM((nt * nx, 8, LANES), f32),
-            pltpu.VMEM((8, width), f32),
             pltpu.VMEM((samples, 8, width), f32),
             pltpu.VMEM((samples, 8, width), f32),
             pltpu.VMEM((samples, tokens, LANES), f32),
@@ -624,12 +672,13 @@
             pltpu.VMEM((samples, nsp, ctx_local, LANES), bf16),
             pltpu.VMEM((samples, HEAD + 16, keys), bf16),
             pltpu.VMEM((8, 4 * WINDOW), f32),
-            pltpu.VMEM((chunk // WINDOW, ctx + 3 * WINDOW, 4 * WINDOW), f32),
-            pltpu.VMEM((chunk // WINDOW, ctx + 3 * WINDOW, 4 * WINDOW), f32),
+            pltpu.VMEM((nt * samples, chunk // WINDOW, 3 * WINDOW, 4 * WINDOW), f32),
+            pltpu.VMEM((nt * samples, chunk // WINDOW, 8, 4 * WINDOW), f32),
+            pltpu.VMEM((chunk // WINDOW, ctx, 4 * WINDOW), f32),
+            pltpu.VMEM((chunk // WINDOW, ctx, 4 * WINDOW), f32),
             pltpu.VMEM((chunk // WINDOW, 8, 4 * WINDOW), f32),
             pltpu.VMEM((chunk // WINDOW, 8, 4 * WINDOW), f32),
             pltpu.VMEM((samples, tokens, 2 * LANES), bf16),
-            pltpu.VMEM((nt, samples, chunk, 2 * LANES), bf16),
             dma((14,)),
             dma((8,)),
             dma((2, nz)),
@@ -641,13 +690,22 @@
             dma((nt - 1, samples)),
         ],
         compiler_params=pltpu.CompilerParams(
-            collective_id=0, has_side_effects=True, vmem_limit_bytes=61 * 1024 * 1024
+            collective_id=0, has_side_effects=True, vmem_limit_bytes=56 * 1024 * 1024
         ),
         name="layer",
     )(
         latent, context, condition, ctx_cond.reshape(1, feats), norm_gain.reshape(1, width), w_shift, w_scale, w_gate,
         w_query, w_key.T, w_value.T, w_out, sink_logit.reshape(1, 4), ctx_lift.reshape(1, 4),
     )
+    return pl.pallas_call(
+        closing,
+        out_shape=jax.ShapeDtypeStruct((samples, chunk, width), bf16),
+        in_specs=[vmem] * 4,
+        out_specs=anywhere,
+        scratch_shapes=[pltpu.VMEM((chunk, width), bf16), dma((5,))],
+        compiler_params=pltpu.CompilerParams(vmem_limit_bytes=16 * 1024 * 1024),
+        name="closing",
+    )(*kept)
 
 
 def solution(mesh):

time: 49.8 us -> 48.1 us (0.966); the launches traced: 49.1 us -> 48 us
  local copies, waits for them, and re-layouts: 1.32 us -> 0 us
    unnamed x1 -> x0, local copies, waits for them, and re-layouts: 1.32 us -> none
    pallas_call x1 -> x2, Pallas kernels: 47.7 us -> 47.9 us  [the longest x1 45.9 us: shards(): pl.pallas_call(functools.partial(layer, sizes), out_shape=(pltpu.VMEM((ch...]
where the time goes in v5:
time: 48.1 us; the launch traced here: 48 us
  Pallas kernels  47.9 us (100%)
    pallas_call x1, Pallas kernels, shards(): pl.pallas_call(functools.partial(layer, sizes), out_shape=(pltpu.VMEM((ch...  45.9 us
    pallas_call x1, Pallas kernels, shards(): pl.pallas_call(closing, out_shape=jax.ShapeDtypeStruct((samples, chunk, w...  2 us

profile of v5, /device:TPU:32, one launch (start us, length us, event | category | flops | bytes accessed | tf_op | source)
XLA Modules:
  0.0 48.0 jit_solution(18430625717848776334)
XLA Ops:
  0.0 45.9 %layer.1 = (bf16[256,2048]{1,0:T(8,128)(2,1)S(1)}, bf16[4,2,256,256]{3,2,1,0:T(8,128)(2,1)S(1)}, bf16[1024,2048]{1,0:T(8,128)(2,1)S(1)}, f32[8,2048]{1,0:T(8,128)S(1)}) custom-call(bf16[2,1024,2048]{2,1,0:T(8,128)(2,1)} %x_hbm.1, bf16[2,32,2048]{2,1,0:T(8,128)(2,1)} %context_hbm.1, bf16[2,64]{1,0:T(2,128)(2,1)} %condition_hbm.1, bf16[1,64]{1,0:T(2,128)(2,1)} %bitcast.9, ...), custom_call_target="tpu_custom_call" | custom-call | tf_op jit(solution)/shard_map/layer/pallas_call | solution.py:637
  45.9 2.0 %closing.1 = bf16[2,256,2048]{2,1,0:T(8,128)(2,1)} custom-call(bf16[256,2048]{1,0:T(8,128)(2,1)S(1)} %get-tuple-element.9.first_v, bf16[4,2,256,256]{3,2,1,0:T(8,128)(2,1)S(1)} %get-tuple-element.10.by_v, bf16[1024,2048]{1,0:T(8,128)(2,1)S(1)} %get-tuple-element.11.wo_v, f32[8,2048]{1,0:T(8,128)S(1)} %get-tuple-element.12.modr_v), custom_call_target="tpu_custom_call" | custom-call | tf_op jit(solution)/shard_map/closing/pallas_call | solution.py:700

commit v6 on v5

--- a/solution.py
+++ b/solution.py
@@ -583,17 +583,17 @@
         return carry
 
     lax.fori_loop(0, turns - 1, chunk_step, 0)
-    both([weights(turns - 1, buffers[(turns - 1) % 2], sub) for sub in range(subs)], None, None, None)
-    by_v[tp] = att_v[:, pl.ds(pl.multiple_of(tp * chunk, chunk), chunk), :]
-
+    own = pl.ds(pl.multiple_of(tp * chunk, chunk), chunk)
+    by_v[tp, 0] = att_v[0, own, :]
     for k in (6, 7, 8):
         wo_sends[k].wait_recv()
     for k in range(nt - 1):
         att_copy(k, 0).wait_recv()
+    both([weights(turns - 1, buffers[(turns - 1) % 2], sub) for sub in range(subs)], None, None, None)
     out_v[...] = gated(by_v, wo_v, modr_v, 0, slice(0, width))
-    for sample in range(1, samples):
-        for k in range(nt - 1):
-            att_copy(k, sample).wait_recv()
+    by_v[tp, 1] = att_v[1, own, :]
+    for k in range(nt - 1):
+        att_copy(k, 1).wait_recv()
 
     drain(rx_v, stage_sem.at[0])
     drain(rz_v, stage_sem.at[2])

time: 48.1 us -> 48.9 us (1.017); the launches traced: 48 us -> 48.4 us
  no operation moved by 1% of the time
where the time goes in v6:
time: 48.9 us; the launch traced here: 48.4 us
  Pallas kernels  48.2 us (99%)
    pallas_call x1, Pallas kernels, shards(): pl.pallas_call(functools.partial(layer, sizes), out_shape=(pltpu.VMEM((ch...  46.2 us
    pallas_call x1, Pallas kernels, shards(): pl.pallas_call(closing, out_shape=jax.ShapeDtypeStruct((samples, chunk, w...  2 us

profile of v6, /device:TPU:32, one launch (start us, length us, event | category | flops | bytes accessed | tf_op | source)
XLA Modules:
  0.0 48.4 jit_solution(13124669466244968924)
XLA Ops:
  0.0 46.2 %layer.1 = (bf16[256,2048]{1,0:T(8,128)(2,1)S(1)}, bf16[4,2,256,256]{3,2,1,0:T(8,128)(2,1)S(1)}, bf16[1024,2048]{1,0:T(8,128)(2,1)S(1)}, f32[8,2048]{1,0:T(8,128)S(1)}) custom-call(bf16[2,1024,2048]{2,1,0:T(8,128)(2,1)} %x_hbm.1, bf16[2,32,2048]{2,1,0:T(8,128)(2,1)} %context_hbm.1, bf16[2,64]{1,0:T(2,128)(2,1)} %condition_hbm.1, bf16[1,64]{1,0:T(2,128)(2,1)} %bitcast.9, ...), custom_call_target="tpu_custom_call" | custom-call | tf_op jit(solution)/shard_map/layer/pallas_call | solution.py:637
  46.2 2.0 %closing.1 = bf16[2,256,2048]{2,1,0:T(8,128)(2,1)} custom-call(bf16[256,2048]{1,0:T(8,128)(2,1)S(1)} %get-tuple-element.9.first_v, bf16[4,2,256,256]{3,2,1,0:T(8,128)(2,1)S(1)} %get-tuple-element.10.by_v, bf16[1024,2048]{1,0:T(8,128)(2,1)S(1)} %get-tuple-element.11.wo_v, f32[8,2048]{1,0:T(8,128)S(1)} %get-tuple-element.12.modr_v), custom_call_target="tpu_custom_call" | custom-call | tf_op jit(solution)/shard_map/closing/pallas_call | solution.py:700
